TPU v7x, 32 devices: a whole 2x2x4 slice. The times are simulated.
32 devices in a mesh: grp: 2 (over y), sp: 4 (over z), tp: 4 (over x, core).
Axes of the slice: x: 2, y: 2, z: 4, core: 2. Of those that a mesh axis runs over, the one named last changes fastest.
Arguments:
- tokens: bfloat16 [1024, 2048], P(('grp', 'sp'), 'tp'), parts along dimension 0, may hold values from -6 to 6
- norm_gain: float32 [2048], replicated, may hold values from 0.1 to 1.9
- att_q_weight: bfloat16 [1024, 2048], P('tp', 'sp'), may hold values from -0.625 to 0.625
- att_k_weight: bfloat16 [512, 2048], P('tp', 'sp'), may hold values from -0.125 to 0.125
- att_v_weight: bfloat16 [512, 2048], P('tp', 'sp'), may hold values from -0.125 to 0.125
- rec_q_weight: bfloat16 [1024, 2048], P('tp', 'sp'), may hold values from -0.125 to 0.125
- rec_f_weight: bfloat16 [1024, 2048], P('tp', 'sp'), may hold values from -0.125 to 0.125
- rec_i_weight: bfloat16 [1024, 2048], P('tp', 'sp'), may hold values from -0.125 to 0.125
- att_out_weight: bfloat16 [1024, 2048], P('tp', 'sp'), may hold values from -1.5 to 1.5
- rec_out_weight: bfloat16 [1024, 2048], P('tp', 'sp'), may hold values from -0.1875 to 0.1875
- score_offset: float32 [16], P('tp'), may hold values from -11.5 to -3
- lower_bound: float32 [1024], P('tp'), may hold values from 0.94 to 0.99999
- decay_shift: float32 [1024, 1024], P(('grp', 'sp'), 'tp'), parts along dimension 0, may hold values from -2.1 to 0
- rec_gain: float32 [1024], P('tp'), may hold values from 0.1 to 1.9
Outputs:
- mixed: bfloat16 [1024, 2048], P(('grp', 'sp', 'tp')), parts along dimension 0
There are 2 independent parts, one for each index of `grp`. A program takes and returns all parts, laid end to end along the dimension named above; an argument that names none is the same for every part. Nothing has to cross between parts.
All inputs are finite; a program needn't handle non-finite values.
Results may differ from a plain program's by a relative error of at most 0.015.
Values may be sent and summed in bfloat16 or wider, within the bound.
A program may use at most 64 MiB of HBM per device.

v0:
```python
import functools

import jax
import jax.numpy as jnp
from jax import lax
from jax.experimental import pallas as pl
from jax.experimental.pallas import tpu as pltpu
from jax.sharding import PartitionSpec as P

HEAD = 64
REC_KEY = 128
REC_VAL = 128
SPAN = 64


EPS = 1e-06
TOP_PRECISION = lax.Precision.HIGHEST


def entering(x, axis, combine, identity):
    count, here = (lax.axis_size(axis), lax.axis_index(axis))
    everything = jax.tree.map(
        lambda part, kind: lax.all_gather(part.astype(kind), axis), x, (jnp.bfloat16, jnp.bfloat16)
    )
    start = jax.tree.map(
        lambda part, zero: jnp.broadcast_to(jnp.asarray(zero, part.dtype), part.shape), x, identity
    )

    def entering_turn(k, before):
        reached = k < here
        new = combine(
            before, jax.tree.map(lambda part, own: part[k].astype(own.dtype), everything, x)
        )
        return jax.tree.map(lambda a, b: jnp.where(reached, a, b), new, before)

    return lax.fori_loop(0, count, entering_turn, start)


def make_fold(norm_gain, weights, carry, piece):
    elementwise_sq, totals = carry
    raw = piece.astype(jnp.float32)
    scaled = (raw * norm_gain[None, :]).astype(jnp.bfloat16)
    elementwise_sq = jnp.sum(raw * raw, axis=1)
    updated = []
    for total, weight in zip(totals, weights):
        updated.append(
            lax.dot_general(
                scaled, weight, (((1,), (1,)), ((), ())), preferred_element_type=jnp.float32
            )
        )
    return (elementwise_sq, tuple(updated))


def project_all(tokens, norm_gain, weights):
    rows = tokens.shape[0]
    width = weights[0].shape[1]
    start_carry = (
        jnp.zeros((rows,), jnp.float32),
        tuple((jnp.zeros((rows, weight.shape[0]), jnp.float32) for weight in weights)),
    )
    elementwise_sq, totals = make_fold(
        norm_gain, weights, start_carry, lax.all_gather(tokens, "tp", axis=1, tiled=True)
    )
    inv_rms = lax.rsqrt(elementwise_sq / width + EPS)
    return tuple((total * inv_rms[:, None] for total in totals))


def attention(att_query, key_value, score_offset):
    rows = att_query.shape[0]
    gathered = lax.all_gather(key_value, "sp", axis=0, tiled=True)
    seq = gathered.shape[0]
    kv_heads = key_value.shape[1] // (2 * HEAD)
    q_heads = att_query.shape[1] // HEAD
    group = q_heads // kv_heads
    kv_width = kv_heads * HEAD
    queries = att_query.reshape(rows, kv_heads, group, HEAD)
    offsets = score_offset.reshape(kv_heads, group)
    kblock = min(1024, seq)
    first_row = lax.axis_index("sp") * rows
    query_pos = first_row + jnp.arange(rows, dtype=jnp.int32)
    count = (first_row + rows - 1) // kblock + 1

    def attention_turn(step, carry):
        summed, run = carry
        block_start = (count - 1 - step) * kblock
        block = lax.dynamic_slice_in_dim(gathered, block_start, kblock, 0)
        keys = block[:, :kv_width].reshape(kblock, kv_heads, HEAD)
        values = block[:, kv_width:].reshape(kblock, kv_heads, HEAD)
        score = (
            jnp.einsum("tkgd,skd->tkgs", queries, keys, preferred_element_type=jnp.float32)
            * HEAD ** (-0.5)
            + offsets[None, :, :, None]
        )
        key_pos = block_start + jnp.arange(kblock, dtype=jnp.int32)
        visible = (key_pos[None, :] < query_pos[:, None])[:, None, None, :]
        keep = jnp.where(visible, jax.nn.log_sigmoid(-score), 0.0)
        tail = lax.cumsum(keep, axis=3, reverse=True) - keep
        weight = jnp.where(
            visible, jnp.exp(jax.nn.log_sigmoid(score) + tail + run[..., None]), 0.0
        ).astype(jnp.bfloat16)
        summed = summed + jnp.einsum(
            "tkgs,skd->tkgd", weight, values, preferred_element_type=jnp.float32
        )
        return (summed, run + jnp.sum(keep, axis=3))

    start_carry = (
        jnp.zeros((rows, kv_heads, group, HEAD), jnp.float32),
        jnp.zeros((rows, kv_heads, group), jnp.float32),
    )
    summed, _ = lax.fori_loop(0, count, attention_turn, start_carry)
    return summed.reshape(rows, q_heads * HEAD).astype(jnp.bfloat16)


def block_pass(carry, inputs):
    state_matrix, prefix = carry
    query_rows, log_decay, keyed_values, value_rows = inputs
    span = query_rows.shape[0]
    cumulative_log = jnp.cumsum(log_decay, axis=0)
    lower = jnp.arange(span, dtype=jnp.int32)[:, None] >= jnp.arange(span, dtype=jnp.int32)[None, :]
    diff = cumulative_log[:, None] - cumulative_log[None, :]
    decay = jnp.exp(jnp.where(lower[:, :, None, None], diff, -jnp.inf))
    score = jnp.einsum(
        "thk,tshk,shk->ths", query_rows, decay, keyed_values, precision=TOP_PRECISION
    )
    inner = jnp.einsum("ths,shv->thv", score, value_rows, precision=TOP_PRECISION)
    outer_product = jnp.einsum(
        "ril,ilc->ric", query_rows * jnp.exp(cumulative_log), state_matrix, precision=TOP_PRECISION
    )
    final_state = cumulative_log[-1]
    state_matrix = state_matrix * jnp.exp(final_state)[:, :, None] + jnp.einsum(
        "iag,iax->agx",
        keyed_values * jnp.exp(final_state[None] - cumulative_log),
        value_rows,
        precision=TOP_PRECISION,
    )
    reach_limit = query_rows * jnp.exp(cumulative_log + prefix[None])
    return ((state_matrix, prefix + final_state), (inner + outer_product, reach_limit))


def chain(earlier, later):
    return (earlier[0] * later[0], earlier[1] * later[0][:, :, None] + later[1])


def recurrence(rec_query, rec_forget, rec_input, lower_bound, decay_shift, rec_gain):
    rows = rec_query.shape[0]
    heads = rec_gain.shape[0] // REC_VAL
    logit = rec_forget.astype(jnp.float32)
    gap = 1.0 - lower_bound
    log_decay = jnp.log(lower_bound + gap * jax.nn.sigmoid(logit)) + decay_shift
    keyed_values = gap * jax.nn.sigmoid(-logit)
    query_rows = jax.nn.silu(rec_query.astype(jnp.float32))
    blocks = rows // SPAN

    def split(array, depth):
        return array.reshape(blocks, SPAN, heads, depth)

    start_carry = (
        jnp.zeros((heads, REC_KEY, REC_VAL), jnp.float32),
        jnp.zeros((heads, REC_KEY), jnp.float32),
    )
    (state_matrix, total), (local, reach_limit) = lax.scan(
        block_pass,
        start_carry,
        (
            split(query_rows, REC_KEY),
            split(log_decay, REC_KEY),
            split(keyed_values, REC_KEY),
            split(rec_input.astype(jnp.float32), REC_VAL),
        ),
    )
    identity = (
        jnp.ones((heads, REC_KEY), jnp.float32),
        jnp.zeros((heads, REC_KEY, REC_VAL), jnp.float32),
    )
    incoming_state = entering((jnp.exp(total), state_matrix), "sp", chain, identity)
    running_memory = jnp.einsum(
        "lida,dao->lido", reach_limit, incoming_state[1], precision=TOP_PRECISION
    )
    rec_raw = (local + running_memory).reshape(rows, heads, REC_VAL)
    rescaled_input = (
        rec_raw
        * lax.rsqrt(jnp.mean(rec_raw * rec_raw, axis=2, keepdims=True) + EPS)
        * rec_gain.reshape(heads, REC_VAL)
    )
    return rescaled_input.reshape(rows, heads * REC_VAL).astype(jnp.bfloat16)


def gathered_plan(
    tokens,
    norm_gain,
    att_q_weight,
    att_k_weight,
    att_v_weight,
    rec_q_weight,
    rec_f_weight,
    rec_i_weight,
    att_out_weight,
    rec_out_weight,
    score_offset,
    lower_bound,
    decay_shift,
    rec_gain,
):
    inputs = (
        lax.all_gather(att_q_weight, "sp", axis=1, tiled=True),
        lax.all_gather(att_k_weight, "sp", axis=1, tiled=True),
        lax.all_gather(att_v_weight, "sp", axis=1, tiled=True),
        lax.all_gather(rec_q_weight, "sp", axis=1, tiled=True),
        lax.all_gather(rec_f_weight, "sp", axis=1, tiled=True),
        lax.all_gather(rec_i_weight, "sp", axis=1, tiled=True),
    )
    projected = project_all(tokens, norm_gain, inputs)
    att_query = projected[0].astype(jnp.bfloat16)
    key_value = jnp.concatenate(projected[1:3], axis=1).astype(jnp.bfloat16)
    rec_query = projected[3].astype(jnp.bfloat16)
    rec_forget = projected[4].astype(jnp.bfloat16)
    rec_input = projected[5].astype(jnp.bfloat16)
    att_out = attention(att_query, key_value, score_offset)
    rec_out = recurrence(rec_query, rec_forget, rec_input, lower_bound, decay_shift, rec_gain)
    outputs = (
        lax.all_gather(att_out_weight, "sp", axis=1, tiled=True),
        lax.all_gather(rec_out_weight, "sp", axis=1, tiled=True),
    )
    att_rows, rec_rows = outputs
    return lax.psum_scatter(
        (
            jnp.dot(att_out, att_rows, preferred_element_type=jnp.float32)
            + jnp.dot(rec_out, rec_rows, preferred_element_type=jnp.float32)
        ).astype(jnp.bfloat16),
        "tp",
        scatter_dimension=0,
        tiled=True,
    )


MESH = pl.DeviceIdType.MESH
STEP = 32


def dot_nt(a, b):
    return lax.dot_general(a, b, (((1,), (1,)), ((), ())), preferred_element_type=jnp.float32)


def dot_tn(a, b):
    return lax.dot_general(a, b, (((0,), (0,)), ((), ())), preferred_element_type=jnp.float32)


def dot_nn(a, b):
    return jnp.dot(a, b, preferred_element_type=jnp.float32)


def remote(src, dst, send_sem, recv_sem, target):
    return pltpu.make_async_remote_copy(
        src_ref=src,
        dst_ref=dst,
        send_sem=send_sem,
        recv_sem=recv_sem,
        device_id=target,
        device_id_type=MESH,
    )


SUB = 32
LAG = 3.5


def stick_block(q, j, group, x, offset_ref):
    block = 128
    low = lax.broadcasted_iota(jnp.int32, (block, block), 0)
    high = lax.broadcasted_iota(jnp.int32, (block, block), 1)
    later = (low > high).astype(jnp.bfloat16)
    visible = jnp.concatenate([high < low] * group, axis=0)
    offset = jnp.concatenate(
        [jnp.full((block, block), offset_ref[j * group + g], jnp.float32) for g in range(group)],
        axis=0,
    )
    queries = x[q * block:(q + 1) * block, :group * HEAD]
    queries = jnp.concatenate([queries[:, g * HEAD:(g + 1) * HEAD] for g in range(group)], axis=0)
    run = jnp.zeros((group * block, 1), jnp.float32)
    summed = jnp.zeros((group * block, HEAD), jnp.float32)
    for c in range(q, -1, -1):
        keys = x[c * block:(c + 1) * block, group * HEAD:(group + 1) * HEAD]
        values = x[c * block:(c + 1) * block, (group + 1) * HEAD:(group + 2) * HEAD]
        score = dot_nt(queries, keys) * HEAD ** (-0.5) + offset
        keep = -(jnp.maximum(score, 0.0) + jnp.log1p(jnp.exp(-jnp.abs(score))))
        gate = score + keep
        if c == q:
            keep = jnp.where(visible, keep, 0.0)
        top = keep.astype(jnp.bfloat16)
        rest = (keep - top.astype(jnp.float32)).astype(jnp.bfloat16)
        tail = dot_nn(top, later) + dot_nn(rest, later)
        weight = jnp.exp(gate + tail + run)
        if c == q:
            weight = jnp.where(visible, weight, 0.0)
        summed = summed + dot_nn(weight.astype(jnp.bfloat16), values)
        run = run + jnp.sum(keep, axis=1, keepdims=True)
    return jnp.concatenate(
        [summed[g * block:(g + 1) * block] for g in range(group)], axis=1
    ).astype(jnp.bfloat16)


def state_block(b, j, x, first, bound_ref, shift_ref, gain_ref, state_ref):
    block = 128
    bound = bound_ref[:, pl.ds(pl.multiple_of(j * REC_KEY, REC_KEY), REC_KEY)]
    gain = gain_ref[:, pl.ds(pl.multiple_of(j * REC_VAL, REC_VAL), REC_VAL)]
    gap = 1.0 - bound
    low = lax.broadcasted_iota(jnp.int32, (block, block), 0)
    high = lax.broadcasted_iota(jnp.int32, (block, block), 1)
    upto = ((high <= low) & (high // STEP == low // STEP)).astype(jnp.float32)
    lower = (
        lax.broadcasted_iota(jnp.int32, (STEP, STEP), 0)
        >= lax.broadcasted_iota(jnp.int32, (STEP, STEP), 1)
    )
    state = jnp.zeros((REC_VAL, REC_KEY), jnp.float32) if b == 0 else state_ref[...]
    at = slice(b * block, (b + 1) * block)
    query = x[at, first:first + REC_KEY].astype(jnp.float32)
    logit = x[at, first + REC_KEY:first + 2 * REC_KEY].astype(jnp.float32)
    value = x[at, first + 2 * REC_KEY:first + 2 * REC_KEY + REC_VAL]
    log_decay = jnp.log(bound + gap * jax.nn.sigmoid(logit)) + shift_ref[at]
    keyed = gap * jax.nn.sigmoid(-logit)
    query = query * jax.nn.sigmoid(query)
    running = jnp.dot(upto, log_decay, precision=TOP_PRECISION, preferred_element_type=jnp.float32)
    outs = []
    for i in range(block // STEP):
        it = slice(i * STEP, (i + 1) * STEP)
        cumulative, q, k, v = running[it], query[it], keyed[it], value[it]
        middle = cumulative[STEP // 2 - 1:STEP // 2]
        last = cumulative[STEP - 1:STEP]
        score = dot_nt(
            (q * jnp.exp(cumulative - middle)).astype(jnp.bfloat16),
            (k * jnp.exp(middle - cumulative)).astype(jnp.bfloat16),
        )
        score = jnp.where(lower, score, 0.0).astype(jnp.bfloat16)
        raw = dot_nn(score, v) + dot_nt(
            (q * jnp.exp(cumulative)).astype(jnp.bfloat16), state.astype(jnp.bfloat16)
        )
        state = state * jnp.exp(last) + dot_tn(
            v, (k * jnp.exp(last - cumulative)).astype(jnp.bfloat16)
        )
        scale = lax.rsqrt(jnp.mean(raw * raw, axis=1, keepdims=True) + EPS)
        outs.append((raw * scale * gain).astype(jnp.bfloat16))
    state_ref[...] = state
    return jnp.concatenate(outs, axis=0)


def layer_kernel(
    n, nt, group,
    tok_ref, gain_ref, aq_ref, ak_ref, av_ref, rq_ref, rf_ref, ri_ref, shift_ref,
    wa_ref, wr_ref, offset_ref, bound_ref, rec_gain_ref,
    out_ref,
    tbuf, shifts, squares, part, sent, came, x, state, heads, shares, landed, mixed,
    a_send, a_recv, a_local, b_send, b_recv, d_send, d_recv, d_local, q_send, q_recv,
    c_send, c_recv, e_send, e_recv, f_send, f_recv, g_send, g_recv, g_local,
):
    s, t = lax.axis_index("sp"), lax.axis_index("tp")
    rows, feats = tok_ref.shape
    piece = rows // nt
    width = x.shape[1]
    att_width = (group + 2) * HEAD
    wide = group * HEAD
    cols = wa_ref.shape[1]
    subs = rows // SUB
    ends = (0, n - 1)
    at_end = (s == 0) | (s == n - 1)
    e = s // (n - 1)
    f32, bf16 = jnp.float32, jnp.bfloat16

    barrier = pltpu.get_barrier_semaphore()
    for a in range(n):
        for b in range(nt):
            if a or b:
                pl.semaphore_signal(
                    barrier, inc=1,
                    device_id={"sp": lax.rem(s + a, n), "tp": lax.rem(t + b, nt)},
                    device_id_type=MESH,
                )
    pl.semaphore_wait(barrier, n * nt - 1)

    def first_copy(j):
        return remote(
            tok_ref.at[pl.ds(j * piece, piece)], tbuf.at[s, j], a_send.at[j], a_recv.at[s],
            {"sp": t, "tp": j},
        )

    def first_here(j):
        return pltpu.make_async_copy(
            tok_ref.at[pl.ds(j * piece, piece)], tbuf.at[s, j], a_local
        )

    for j in range(nt):
        here = (s == t) & (t == j)
        pl.when(jnp.logical_not(here))(lambda j=j: first_copy(j).start())
        pl.when(here)(lambda j=j: first_here(j).start())

    def shift_copy(i):
        return remote(
            shift_ref.at[:, pl.ds(i * REC_KEY, REC_KEY)], shifts.at[pl.ds(s * rows, rows)],
            d_send.at[i], d_recv.at[s], {"sp": ends[i]},
        )

    def shift_here(i):
        return pltpu.make_async_copy(
            shift_ref.at[:, pl.ds(i * REC_KEY, REC_KEY)], shifts.at[pl.ds(s * rows, rows)], d_local
        )

    def second_copy(k, d):
        return remote(
            tbuf.at[k, t], tbuf.at[k, t], b_send.at[k, d], b_recv.at[k, d],
            {"tp": lax.rem(t + d, nt)},
        )

    def relay(k):
        here = (s == k) & (t == k)

        def arrived():
            remote(
                tok_ref.at[pl.ds(0, piece)], tbuf.at[k, t], a_send.at[0], a_recv.at[k],
                {"sp": t, "tp": t},
            ).wait_recv()

        pl.when(jnp.logical_not(here))(arrived)
        pl.when(here)(lambda: first_here(k).wait())
        for d in range(1, nt):
            second_copy(k, d).start()

    gain = gain_ref[:, pl.ds(pl.multiple_of(s * feats, feats), feats)]

    def square_copy(k, i):
        return remote(
            squares.at[s, k], squares.at[s, k], q_send.at[k, i], q_recv.at[s, k], {"sp": ends[i]}
        )

    def chain_copy(i, c):
        to = jnp.maximum(s - 1, 0) if i == 0 else jnp.minimum(s + 1, n - 1)
        return remote(
            sent.at[i, pl.ds(c * SUB, SUB)], came.at[i, pl.ds(c * SUB, SUB)],
            c_send.at[i, c], c_recv.at[i, c], {"sp": to},
        )

    weights = []
    for i in range(2):
        weights.append(jnp.concatenate(
            [
                aq_ref[pl.ds(i * wide, wide)],
                ak_ref[pl.ds(i * HEAD, HEAD)],
                av_ref[pl.ds(i * HEAD, HEAD)],
                rq_ref[pl.ds(i * REC_KEY, REC_KEY)],
                rf_ref[pl.ds(i * REC_KEY, REC_KEY)],
                ri_ref[pl.ds(i * REC_VAL, REC_VAL)],
            ],
            axis=0,
        ))

    def project(k):
        for d in range(1, nt):
            second_copy(k, d).wait_recv()
        raw = tbuf[k].reshape(rows, feats).astype(f32)
        scaled = (raw * gain).astype(bf16)
        for i in range(2):
            product = dot_nt(scaled, weights[i])
            part[i, pl.ds(k * rows, rows)] = product

            @pl.when(s == ends[1 - i])
            def _():
                for r in range(subs):
                    c = k * subs + r
                    sent[i, pl.ds(c * SUB, SUB)] = product[r * SUB:(r + 1) * SUB].astype(bf16)
                    chain_copy(i, c).start()

        total = jnp.sum(raw * raw, axis=1, keepdims=True)
        flat = jnp.transpose(jnp.broadcast_to(total, (rows, 128)))
        squares[s, k] = flat[:8]
        for i in range(2):
            pl.when(s != ends[i])(lambda i=i: square_copy(k, i).start())

    def forward(i, c):
        chain_copy(i, c).wait_recv()
        at = (i, pl.ds(c * SUB, SUB))
        sent[at] = (part[at] + came[at].astype(f32)).astype(bf16)
        chain_copy(i, c).start()

    def head_copy(i, k, to):
        at = (i, pl.ds(k * rows, rows))
        return remote(
            heads.at[at], heads.at[at], e_send.at[k, to], e_recv.at[i, k], {"sp": to}
        )

    def mix(k):
        span = pl.ds(k * rows, rows)
        for i in range(2):
            @pl.when(s == ends[i])
            def _():
                for r in range(subs):
                    chain_copy(i, k * subs + r).wait_recv()
                for v in range(n):
                    if v != ends[i]:
                        remote(
                            squares.at[v, k], squares.at[v, k], q_send.at[k, i], q_recv.at[v, k],
                            {"sp": v},
                        ).wait_recv()
                if k == ends[i]:
                    shift_here(i).wait()
                else:
                    remote(
                        shift_ref.at[:, pl.ds(i * REC_KEY, REC_KEY)], shifts.at[span],
                        d_send.at[i], d_recv.at[k], {"sp": k},
                    ).wait_recv()
        total = squares[0, k, :1]
        for v in range(1, n):
            total = total + squares[v, k, :1]
        inv_rms = lax.rsqrt(total / gain_ref.shape[1] + EPS)
        inv_rms = jnp.transpose(jnp.broadcast_to(inv_rms, (128, rows)))
        for c in range(width // 128):
            lane = pl.ds(c * 128, 128)
            result = part[e, span, lane] + came[e, span, lane].astype(f32)
            x[span, lane] = (result * inv_rms).astype(bf16)
        heads[e, span, pl.ds(0, wide)] = stick_block(k, e, group, x, offset_ref)
        heads[e, span, pl.ds(wide, REC_VAL)] = state_block(
            k, e, x, att_width, bound_ref, shifts, rec_gain_ref, state
        )
        for i in range(2):
            @pl.when(s == ends[i])
            def _():
                for to in (range(n - 1, 0, -1) if i == 0 else range(n - 1)):
                    head_copy(i, k, to).start()

    def share_copy(k, b):
        to = lax.rem(t + b, nt)
        return remote(
            shares.at[k, to], landed.at[k, b], f_send.at[k, b], f_recv.at[k, b], {"tp": to}
        )

    def multiply(k):
        span = pl.ds(k * rows, rows)
        total = None
        for i in range(2):
            pl.when(s != ends[i])(lambda i=i: head_copy(i, k, ends[i]).wait_recv())
        for i in range(2):
            for ref, first, size in ((wa_ref, 0, wide), (wr_ref, wide, REC_VAL)):
                term = dot_nn(heads[i, span, pl.ds(first, size)], ref[pl.ds(i * size, size)])
                total = term if total is None else total + term
        shares[k] = total.astype(bf16).reshape(nt, piece, cols)
        for b in range(1, nt):
            share_copy(k, b).start()

    place = out_ref.at[:, pl.ds(pl.multiple_of(s * cols, cols), cols)]

    def final_copy(k):
        return remote(mixed.at[k], place, g_send.at[k], g_recv.at[s], {"sp": k})

    def final_here(k):
        return pltpu.make_async_copy(mixed.at[k], place, g_local)

    def combine(k):
        result = shares[k, t].astype(f32)
        for b in range(1, nt):
            share_copy(k, b).wait_recv()
            result = result + landed[k, b].astype(f32)
        mixed[k] = result.astype(bf16)
        pl.when(s != k)(lambda: final_copy(k).start())
        pl.when(s == k)(lambda: final_here(k).start())

    relay(0)
    for k in range(n):
        if k + 1 < n:
            relay(k + 1)
        project(k)
        if k == 0:
            for i, u in enumerate(ends):
                pl.when(s != u)(lambda i=i: shift_copy(i).start())
                pl.when(s == u)(lambda i=i: shift_here(i).start())

    for v in range(1, n - 1):
        events = [(c + LAG * v, 1, c) for c in range(n * subs)]
        events += [(c + LAG * (n - 1 - v), 0, c) for c in range(n * subs)]

        @pl.when(s == v)
        def _():
            for _, i, c in sorted(events):
                forward(i, c)

    @pl.when(at_end)
    def _():
        for k in range(n - 1):
            mix(k)

    multiply(0)

    @pl.when(at_end)
    def _():
        mix(n - 1)

    for k in range(1, n):
        multiply(k)
        combine(k - 1)
    combine(n - 1)

    for v in range(n):
        @pl.when(s != v)
        def _():
            remote(
                mixed.at[0], out_ref.at[:, pl.ds(v * cols, cols)], g_send.at[0], g_recv.at[v],
                {"sp": v},
            ).wait_recv()
        pl.when(s == v)(lambda v=v: final_here(v).wait())

    for j in range(nt):
        here = (s == t) & (t == j)
        pl.when(jnp.logical_not(here))(lambda j=j: first_copy(j).wait_send())
    for i in range(2):
        pl.when(s != ends[i])(lambda i=i: shift_copy(i).wait_send())
    for k in range(n):
        for d in range(1, nt):
            second_copy(k, d).wait_send()
            share_copy(k, d).wait_send()
        for i in range(2):
            pl.when(s != ends[i])(lambda i=i, k=k: square_copy(k, i).wait_send())

            @pl.when(s == ends[i])
            def _():
                for to in range(n):
                    if to != ends[i]:
                        head_copy(i, k, to).wait_send()

            @pl.when(s != ends[i])
            def _():
                for r in range(subs):
                    chain_copy(i, k * subs + r).wait_send()
        pl.when(s != k)(lambda k=k: final_copy(k).wait_send())


def stationary_fits(args):
    n, nt = lax.axis_size("sp"), lax.axis_size("tp")
    tokens, att_q, att_k, rec_i = args[0], args[2], args[3], args[7]
    rows, feats = tokens.shape
    return (
        n == nt
        and n >= 3
        and att_k.shape[0] // HEAD == 2
        and rec_i.shape[0] // REC_VAL == 2
        and (att_q.shape[0] // att_k.shape[0]) * HEAD == 128
        and feats == att_q.shape[1]
        and rows == 128
    )


def stationary(*args):
    n, nt = lax.axis_size("sp"), lax.axis_size("tp")
    tokens, norm_gain, att_q, att_k = args[:4]
    score_offset, lower_bound, decay_shift, rec_gain = args[10:]
    rows, feats = tokens.shape
    seq = rows * n
    cols = args[8].shape[1]
    group = att_q.shape[0] // att_k.shape[0]
    width = (group + 2) * HEAD + 2 * REC_KEY + REC_VAL
    wide = group * HEAD + REC_VAL
    piece = rows // nt
    chunks = seq // SUB
    bf16, f32 = jnp.bfloat16, jnp.float32
    dma = pltpu.SemaphoreType.DMA
    vmem = pl.BlockSpec(memory_space=pltpu.VMEM)
    smem = pl.BlockSpec(memory_space=pltpu.SMEM)
    return pl.pallas_call(
        functools.partial(layer_kernel, n, nt, group),
        out_shape=jax.ShapeDtypeStruct((piece, cols * n), bf16),
        in_specs=[vmem] * 11 + [smem, vmem, vmem],
        out_specs=vmem,
        scratch_shapes=[
            pltpu.VMEM((n, nt, piece, feats), bf16),
            pltpu.VMEM((seq, REC_KEY), f32),
            pltpu.VMEM((n, n, 8, rows), f32),
            pltpu.VMEM((2, seq, width), f32),
            pltpu.VMEM((2, seq, width), bf16),
            pltpu.VMEM((2, seq, width), bf16),
            pltpu.VMEM((seq, width), bf16),
            pltpu.VMEM((REC_VAL, REC_KEY), f32),
            pltpu.VMEM((2, seq, wide), bf16),
            pltpu.VMEM((n, nt, piece, cols), bf16),
            pltpu.VMEM((n, nt, piece, cols), bf16),
            pltpu.VMEM((n, piece, cols), bf16),
            dma((nt,)), dma((n,)), dma, dma((n, nt)), dma((n, nt)), dma((2,)), dma((n,)), dma,
            dma((n, 2)), dma((n, n)), dma((2, chunks)), dma((2, chunks)),
            dma((n, n)), dma((2, n)), dma((n, nt)), dma((n, nt)), dma((n,)), dma((n,)), dma,
        ],
        compiler_params=pltpu.CompilerParams(collective_id=0, has_side_effects=True),
        name="layer",
    )(
        tokens, norm_gain.reshape(1, -1), *args[2:8], decay_shift, args[8], args[9],
        score_offset, lower_bound.reshape(1, -1), rec_gain.reshape(1, -1),
    )


def on_device(*args):
    if stationary_fits(args):
        return stationary(*args)
    return gathered_plan(*args)


def solution(mesh):
    in_specs = (
        P(("grp", "sp"), "tp"),
        P(),
        P("tp", "sp"),
        P("tp", "sp"),
        P("tp", "sp"),
        P("tp", "sp"),
        P("tp", "sp"),
        P("tp", "sp"),
        P("tp", "sp"),
        P("tp", "sp"),
        P("tp"),
        P("tp"),
        P(("grp", "sp"), "tp"),
        P("tp"),
    )
    out_specs = P(("grp", "sp", "tp"), None)
    return jax.shard_map(
        on_device, mesh=mesh, in_specs=in_specs, out_specs=out_specs, check_vma=False
    )
```

profile of v0, /device:TPU:0, one launch (start us, length us, event | category | flops | bytes accessed | tf_op | source)
XLA Modules:
  0.0 64.1 jit_solution(18160280621494979110)
XLA Ops:
  0.0 62.5 %layer.1 = bf16[32,2048]{1,0:T(8,128)(2,1)} custom-call(bf16[128,512]{1,0:T(8,128)(2,1)} %tok_ref.1, f32[1,2048]{1,0:T(1,128)} %bitcast.3, bf16[256,512]{1,0:T(8,128)(2,1)} %aq_ref.1, bf16[128,512]{1,0:T(8,128)(2,1)} %ak_ref.1, bf16[128,512]{1,0:T(8,128)(2,1)} %av_ref.1, bf16[256,512]{1,0:T(8,128)(2,1)} %rq_ref.1, bf16[256,512]{1,0:T(8,128)(2,1)} %rf_ref.1, ...), custom_call_target="tpu_custom_call" | custom-call | tf_op jit(solution)/shard_map/layer/pallas_call | solution.py:663
  62.5 1.6 %copy.16 = bf16[32,2048]{1,0:T(8,128)(2,1)} copy(bf16[32,2048]{1,0:T(8,128)(2,1)} %layer.1) | data formatting | bytes 262144
where the time goes:
time: 64.7 us; the launch traced here: 64.1 us
  Pallas kernels  62.5 us (97%)
  local copies, waits for them, and re-layouts  1.57 us (2%)
    pallas_call x1, Pallas kernels, stationary(): pl.pallas_call(functools.partial(layer_kernel, n, nt, group), out_shape=j...  62.5 us
    unnamed x1, local copies, waits for them, and re-layouts  1.57 us

commit v1 on v0

--- a/solution.py
+++ b/solution.py
@@ -1,3 +1,4 @@
+import contextlib
 import functools
 
 import jax
@@ -261,23 +262,32 @@
 
 
 SUB = 32
-LAG = 3.5
-
-
-def stick_block(q, j, group, x, offset_ref):
+ROWS8 = 8
+LAST = 64
+PROFILE = False
+
+
+def scope(name):
+    return jax.named_scope(name) if PROFILE else contextlib.nullcontext()
+
+
+def stick_block(first, rows, j, group, x, offset_ref):
     block = 128
+    q, base = first // block, first % block
     low = lax.broadcasted_iota(jnp.int32, (block, block), 0)
     high = lax.broadcasted_iota(jnp.int32, (block, block), 1)
     later = (low > high).astype(jnp.bfloat16)
-    visible = jnp.concatenate([high < low] * group, axis=0)
+    row = lax.broadcasted_iota(jnp.int32, (rows, block), 0) + base
+    col = lax.broadcasted_iota(jnp.int32, (rows, block), 1)
+    visible = jnp.concatenate([col < row] * group, axis=0)
     offset = jnp.concatenate(
-        [jnp.full((block, block), offset_ref[j * group + g], jnp.float32) for g in range(group)],
+        [jnp.full((rows, block), offset_ref[j * group + g], jnp.float32) for g in range(group)],
         axis=0,
     )
-    queries = x[q * block:(q + 1) * block, :group * HEAD]
+    queries = x[first:first + rows, :group * HEAD]
     queries = jnp.concatenate([queries[:, g * HEAD:(g + 1) * HEAD] for g in range(group)], axis=0)
-    run = jnp.zeros((group * block, 1), jnp.float32)
-    summed = jnp.zeros((group * block, HEAD), jnp.float32)
+    run = jnp.zeros((group * rows, 1), jnp.float32)
+    summed = jnp.zeros((group * rows, HEAD), jnp.float32)
     for c in range(q, -1, -1):
         keys = x[c * block:(c + 1) * block, group * HEAD:(group + 1) * HEAD]
         values = x[c * block:(c + 1) * block, (group + 1) * HEAD:(group + 2) * HEAD]
@@ -295,24 +305,21 @@
         summed = summed + dot_nn(weight.astype(jnp.bfloat16), values)
         run = run + jnp.sum(keep, axis=1, keepdims=True)
     return jnp.concatenate(
-        [summed[g * block:(g + 1) * block] for g in range(group)], axis=1
+        [summed[g * rows:(g + 1) * rows] for g in range(group)], axis=1
     ).astype(jnp.bfloat16)
 
 
-def state_block(b, j, x, first, bound_ref, shift_ref, gain_ref, state_ref):
-    block = 128
-    bound = bound_ref[:, pl.ds(pl.multiple_of(j * REC_KEY, REC_KEY), REC_KEY)]
-    gain = gain_ref[:, pl.ds(pl.multiple_of(j * REC_VAL, REC_VAL), REC_VAL)]
+def state_block(begin, rows, x, first, bound, gain, shift_ref, state_ref):
     gap = 1.0 - bound
-    low = lax.broadcasted_iota(jnp.int32, (block, block), 0)
-    high = lax.broadcasted_iota(jnp.int32, (block, block), 1)
+    low = lax.broadcasted_iota(jnp.int32, (rows, rows), 0)
+    high = lax.broadcasted_iota(jnp.int32, (rows, rows), 1)
     upto = ((high <= low) & (high // STEP == low // STEP)).astype(jnp.float32)
     lower = (
         lax.broadcasted_iota(jnp.int32, (STEP, STEP), 0)
         >= lax.broadcasted_iota(jnp.int32, (STEP, STEP), 1)
     )
-    state = jnp.zeros((REC_VAL, REC_KEY), jnp.float32) if b == 0 else state_ref[...]
-    at = slice(b * block, (b + 1) * block)
+    state = jnp.zeros((REC_VAL, REC_KEY), jnp.float32) if begin == 0 else state_ref[...]
+    at = slice(begin, begin + rows)
     query = x[at, first:first + REC_KEY].astype(jnp.float32)
     logit = x[at, first + REC_KEY:first + 2 * REC_KEY].astype(jnp.float32)
     value = x[at, first + 2 * REC_KEY:first + 2 * REC_KEY + REC_VAL]
@@ -321,7 +328,7 @@
     query = query * jax.nn.sigmoid(query)
     running = jnp.dot(upto, log_decay, precision=TOP_PRECISION, preferred_element_type=jnp.float32)
     outs = []
-    for i in range(block // STEP):
+    for i in range(rows // STEP):
         it = slice(i * STEP, (i + 1) * STEP)
         cumulative, q, k, v = running[it], query[it], keyed[it], value[it]
         middle = cumulative[STEP // 2 - 1:STEP // 2]
@@ -343,28 +350,61 @@
     return jnp.concatenate(outs, axis=0)
 
 
+def units_of(n, rows):
+    whole = [(k * rows, rows) for k in range(n - 1)]
+    return whole + [((n - 1) * rows + r, LAST) for r in range(0, rows, LAST)]
+
+
 def layer_kernel(
     n, nt, group,
     tok_ref, gain_ref, aq_ref, ak_ref, av_ref, rq_ref, rf_ref, ri_ref, shift_ref,
     wa_ref, wr_ref, offset_ref, bound_ref, rec_gain_ref,
     out_ref,
-    tbuf, shifts, squares, part, sent, came, x, state, heads, shares, landed, mixed,
-    a_send, a_recv, a_local, b_send, b_recv, d_send, d_recv, d_local, q_send, q_recv,
+    tokens, gains, bounds, rec_gains, weights, outs, own_shift, tbuf, shifts, squares, scales,
+    part, sent, came, x, state, heads, shares, landed, mixed,
+    l_sem, a_send, a_recv, a_local, b_send, b_recv, d_send, d_recv, d_local, q_send, q_recv,
     c_send, c_recv, e_send, e_recv, f_send, f_recv, g_send, g_recv, g_local,
 ):
     s, t = lax.axis_index("sp"), lax.axis_index("tp")
-    rows, feats = tok_ref.shape
+    rows, feats = own_shift.shape[0], tokens.shape[-1]
     piece = rows // nt
     width = x.shape[1]
     att_width = (group + 2) * HEAD
     wide = group * HEAD
-    cols = wa_ref.shape[1]
+    cols = outs.shape[-1]
     subs = rows // SUB
     ends = (0, n - 1)
-    at_end = (s == 0) | (s == n - 1)
-    e = s // (n - 1)
     f32, bf16 = jnp.float32, jnp.bfloat16
-
+    units = units_of(n, rows)
+    nu = len(units)
+
+    loads = [
+        pltpu.make_async_copy(tok_ref, tokens, l_sem.at[0]),
+        pltpu.make_async_copy(
+            gain_ref.at[:, pl.ds(pl.multiple_of(s * feats, feats), feats)], gains, l_sem.at[1]
+        ),
+    ]
+    first = 0
+    for ref, size in (
+        (aq_ref, wide), (ak_ref, HEAD), (av_ref, HEAD),
+        (rq_ref, REC_KEY), (rf_ref, REC_KEY), (ri_ref, REC_VAL),
+    ):
+        for i in range(2):
+            loads.append(
+                pltpu.make_async_copy(
+                    ref.at[pl.ds(i * size, size)], weights.at[i, pl.ds(first, size)],
+                    l_sem.at[len(loads)],
+                )
+            )
+        first += size
+    early = len(loads)
+    loads.append(pltpu.make_async_copy(shift_ref, own_shift, l_sem.at[early]))
+    loads.append(pltpu.make_async_copy(bound_ref, bounds, l_sem.at[early + 1]))
+    loads.append(pltpu.make_async_copy(rec_gain_ref, rec_gains, l_sem.at[early + 2]))
+    loads.append(pltpu.make_async_copy(wa_ref, outs.at[0], l_sem.at[early + 3]))
+    loads.append(pltpu.make_async_copy(wr_ref, outs.at[1], l_sem.at[early + 4]))
+
+    loads[0].start()
     barrier = pltpu.get_barrier_semaphore()
     for a in range(n):
         for b in range(nt):
@@ -374,259 +414,381 @@
                     device_id={"sp": lax.rem(s + a, n), "tp": lax.rem(t + b, nt)},
                     device_id_type=MESH,
                 )
-    pl.semaphore_wait(barrier, n * nt - 1)
-
-    def first_copy(j):
-        return remote(
-            tok_ref.at[pl.ds(j * piece, piece)], tbuf.at[s, j], a_send.at[j], a_recv.at[s],
-            {"sp": t, "tp": j},
-        )
-
-    def first_here(j):
-        return pltpu.make_async_copy(
-            tok_ref.at[pl.ds(j * piece, piece)], tbuf.at[s, j], a_local
-        )
-
-    for j in range(nt):
-        here = (s == t) & (t == j)
-        pl.when(jnp.logical_not(here))(lambda j=j: first_copy(j).start())
-        pl.when(here)(lambda j=j: first_here(j).start())
-
-    def shift_copy(i):
-        return remote(
-            shift_ref.at[:, pl.ds(i * REC_KEY, REC_KEY)], shifts.at[pl.ds(s * rows, rows)],
-            d_send.at[i], d_recv.at[s], {"sp": ends[i]},
-        )
-
-    def shift_here(i):
-        return pltpu.make_async_copy(
-            shift_ref.at[:, pl.ds(i * REC_KEY, REC_KEY)], shifts.at[pl.ds(s * rows, rows)], d_local
-        )
-
-    def second_copy(k, d):
-        return remote(
-            tbuf.at[k, t], tbuf.at[k, t], b_send.at[k, d], b_recv.at[k, d],
-            {"tp": lax.rem(t + d, nt)},
-        )
-
-    def relay(k):
-        here = (s == k) & (t == k)
-
-        def arrived():
-            remote(
-                tok_ref.at[pl.ds(0, piece)], tbuf.at[k, t], a_send.at[0], a_recv.at[k],
-                {"sp": t, "tp": t},
-            ).wait_recv()
-
-        pl.when(jnp.logical_not(here))(arrived)
-        pl.when(here)(lambda: first_here(k).wait())
-        for d in range(1, nt):
-            second_copy(k, d).start()
-
-    gain = gain_ref[:, pl.ds(pl.multiple_of(s * feats, feats), feats)]
-
-    def square_copy(k, i):
-        return remote(
-            squares.at[s, k], squares.at[s, k], q_send.at[k, i], q_recv.at[s, k], {"sp": ends[i]}
-        )
-
-    def chain_copy(i, c):
-        to = jnp.maximum(s - 1, 0) if i == 0 else jnp.minimum(s + 1, n - 1)
-        return remote(
-            sent.at[i, pl.ds(c * SUB, SUB)], came.at[i, pl.ds(c * SUB, SUB)],
-            c_send.at[i, c], c_recv.at[i, c], {"sp": to},
-        )
-
-    weights = []
-    for i in range(2):
-        weights.append(jnp.concatenate(
-            [
-                aq_ref[pl.ds(i * wide, wide)],
-                ak_ref[pl.ds(i * HEAD, HEAD)],
-                av_ref[pl.ds(i * HEAD, HEAD)],
-                rq_ref[pl.ds(i * REC_KEY, REC_KEY)],
-                rf_ref[pl.ds(i * REC_KEY, REC_KEY)],
-                ri_ref[pl.ds(i * REC_VAL, REC_VAL)],
-            ],
-            axis=0,
-        ))
-
-    def project(k):
-        for d in range(1, nt):
-            second_copy(k, d).wait_recv()
-        raw = tbuf[k].reshape(rows, feats).astype(f32)
-        scaled = (raw * gain).astype(bf16)
-        for i in range(2):
-            product = dot_nt(scaled, weights[i])
-            part[i, pl.ds(k * rows, rows)] = product
-
-            @pl.when(s == ends[1 - i])
-            def _():
-                for r in range(subs):
-                    c = k * subs + r
-                    sent[i, pl.ds(c * SUB, SUB)] = product[r * SUB:(r + 1) * SUB].astype(bf16)
-                    chain_copy(i, c).start()
-
-        total = jnp.sum(raw * raw, axis=1, keepdims=True)
-        flat = jnp.transpose(jnp.broadcast_to(total, (rows, 128)))
-        squares[s, k] = flat[:8]
-        for i in range(2):
-            pl.when(s != ends[i])(lambda i=i: square_copy(k, i).start())
-
-    def forward(i, c):
-        chain_copy(i, c).wait_recv()
-        at = (i, pl.ds(c * SUB, SUB))
-        sent[at] = (part[at] + came[at].astype(f32)).astype(bf16)
-        chain_copy(i, c).start()
-
-    def head_copy(i, k, to):
-        at = (i, pl.ds(k * rows, rows))
-        return remote(
-            heads.at[at], heads.at[at], e_send.at[k, to], e_recv.at[i, k], {"sp": to}
-        )
-
-    def mix(k):
-        span = pl.ds(k * rows, rows)
-        for i in range(2):
-            @pl.when(s == ends[i])
-            def _():
-                for r in range(subs):
-                    chain_copy(i, k * subs + r).wait_recv()
-                for v in range(n):
-                    if v != ends[i]:
+    for load in loads[1:]:
+        load.start()
+    loads[0].wait()
+    with scope("barrier"):
+        pl.semaphore_wait(barrier, n * nt - 1)
+
+    def plane(v):
+        others = [i for i in range(2) if v != ends[i]]
+        mine = [i for i in range(2) if v == ends[i]]
+        order = (1, 0) if v < n // 2 else (0, 1)
+
+        def parts_of(k):
+            return range(subs) if k == 0 else (slice(None),)
+
+        def slot(c):
+            return 0 if isinstance(c, slice) else c
+
+        def first_copy(c, j):
+            return remote(
+                tokens.at[c, j], tbuf.at[v, c, j], a_send.at[slot(c), j], a_recv.at[v, slot(c)],
+                {"sp": t, "tp": j},
+            )
+
+        def first_here(c):
+            return pltpu.make_async_copy(
+                tokens.at[c, v], tbuf.at[v, c, v], a_local.at[slot(c)]
+            )
+
+        def send_first():
+            for c in parts_of(v):
+                for j in range(nt):
+                    if j == v:
+                        pl.when(t != v)(lambda: first_copy(c, j).start())
+                        pl.when(t == v)(lambda: first_here(c).start())
+                    else:
+                        first_copy(c, j).start()
+
+        def second_copy(k, c, d):
+            return remote(
+                tbuf.at[k, c, t], tbuf.at[k, c, t],
+                b_send.at[k, slot(c), d], b_recv.at[k, slot(c), d],
+                {"tp": lax.rem(t + d, nt)},
+            )
+
+        def relay(k, c):
+            def arrived():
+                remote(
+                    tokens.at[c, 0], tbuf.at[k, c, t], a_send.at[0, 0], a_recv.at[k, slot(c)],
+                    {"sp": (v + 1) % n},
+                ).wait_recv()
+
+            with scope(f"relay{k}"):
+                if k == v:
+                    pl.when(t != v)(arrived)
+                    pl.when(t == v)(lambda: first_here(c).wait())
+                else:
+                    arrived()
+            for d in range(1, nt):
+                second_copy(k, c, d).start()
+
+        def square_copy(k, i):
+            return remote(
+                squares.at[v, k], squares.at[v, k], q_send.at[k, i], q_recv.at[v, k],
+                {"sp": ends[i]},
+            )
+
+        def chain_copy(i, c):
+            to = v - 1 if i == 0 else v + 1
+            return remote(
+                sent.at[i, pl.ds(c * SUB, SUB)], came.at[i, pl.ds(c * SUB, SUB)],
+                c_send.at[i, c], c_recv.at[i, c], {"sp": to},
+            )
+
+        def project(k, c):
+            with scope(f"wtok{k}"):
+                for d in range(1, nt):
+                    second_copy(k, c, d).wait_recv()
+            size = rows if isinstance(c, slice) else SUB
+            begin = k * rows + slot(c) * SUB
+            raw = tbuf[k, c].reshape(size, feats).astype(f32)
+            scaled = (raw * gains[...]).astype(bf16)
+            for i in order:
+                product = dot_nt(scaled, weights[i])
+                if v == ends[1 - i]:
+                    for r in range(size // SUB):
+                        at = begin + r * SUB
+                        sent[i, pl.ds(at, SUB)] = product[r * SUB:(r + 1) * SUB].astype(bf16)
+                        chain_copy(i, at // SUB).start()
+                else:
+                    part[i, pl.ds(begin, size)] = product
+
+        def square(k):
+            raw = tbuf[k].reshape(rows, feats).astype(f32)
+            total = jnp.sum(raw * raw, axis=1, keepdims=True)
+            flat = jnp.transpose(jnp.broadcast_to(total, (rows, 128)))
+            squares[v, k] = flat[:8]
+            for i in others:
+                square_copy(k, i).start()
+
+        def shift_copy(i):
+            return remote(
+                own_shift.at[:, pl.ds(i * REC_KEY, REC_KEY)], shifts.at[pl.ds(v * rows, rows)],
+                d_send.at[i], d_recv.at[v], {"sp": ends[i]},
+            )
+
+        def shift_here(i):
+            return pltpu.make_async_copy(
+                own_shift.at[:, pl.ds(i * REC_KEY, REC_KEY)], shifts.at[pl.ds(v * rows, rows)],
+                d_local,
+            )
+
+        def send_shift():
+            for i in others:
+                shift_copy(i).start()
+            for i in mine:
+                shift_here(i).start()
+
+        def forward(i, c):
+            with scope(f"chain{i}_{c}"):
+                chain_copy(i, c).wait_recv()
+            at = (i, pl.ds(c * SUB, SUB))
+            sent[at] = (part[at] + came[at].astype(f32)).astype(bf16)
+            chain_copy(i, c).start()
+
+        def head_copy(i, u, to):
+            at = (i, pl.ds(units[u][0], units[u][1]))
+            return remote(
+                heads.at[at], heads.at[at], e_send.at[u, to], e_recv.at[i, u], {"sp": to}
+            )
+
+        def near(i):
+            return 1 if i == 0 else n - 2
+
+        def between(i):
+            return [p for p in range(1, n - 1) if p != near(i)]
+
+        def direct(u):
+            return units[u][1] == LAST
+
+        def head_targets(i, u):
+            if v == ends[i]:
+                far = ends[1 - i]
+                if direct(u):
+                    return [far, *between(i), near(i)]
+                return [far, near(i)]
+            if v == near(i) and not direct(u):
+                return between(i)
+            return []
+
+        def send_heads(i, u, to):
+            head_copy(i, u, to).start()
+
+        def wait_heads(i, u):
+            with scope(f"whead{i}_{u}"):
+                head_copy(i, u, ends[i]).wait_recv()
+
+        def mix(u):
+            e = mine[0]
+            begin, size = units[u]
+            k = begin // rows
+            span = pl.ds(begin, size)
+            with scope(f"wmix{u}"):
+                for c in range(begin // SUB, (begin + size) // SUB):
+                    chain_copy(e, c).wait_recv()
+            if begin % rows == 0:
+                for p in range(n):
+                    if p != v:
                         remote(
-                            squares.at[v, k], squares.at[v, k], q_send.at[k, i], q_recv.at[v, k],
-                            {"sp": v},
+                            squares.at[p, k], squares.at[p, k], q_send.at[k, e], q_recv.at[p, k],
+                            {"sp": p},
                         ).wait_recv()
-                if k == ends[i]:
-                    shift_here(i).wait()
+                if k == v:
+                    shift_here(e).wait()
                 else:
                     remote(
-                        shift_ref.at[:, pl.ds(i * REC_KEY, REC_KEY)], shifts.at[span],
-                        d_send.at[i], d_recv.at[k], {"sp": k},
+                        own_shift.at[:, pl.ds(e * REC_KEY, REC_KEY)],
+                        shifts.at[pl.ds(k * rows, rows)], d_send.at[e], d_recv.at[k], {"sp": k},
                     ).wait_recv()
-        total = squares[0, k, :1]
-        for v in range(1, n):
-            total = total + squares[v, k, :1]
-        inv_rms = lax.rsqrt(total / gain_ref.shape[1] + EPS)
-        inv_rms = jnp.transpose(jnp.broadcast_to(inv_rms, (128, rows)))
-        for c in range(width // 128):
-            lane = pl.ds(c * 128, 128)
-            result = part[e, span, lane] + came[e, span, lane].astype(f32)
-            x[span, lane] = (result * inv_rms).astype(bf16)
-        heads[e, span, pl.ds(0, wide)] = stick_block(k, e, group, x, offset_ref)
-        heads[e, span, pl.ds(wide, REC_VAL)] = state_block(
-            k, e, x, att_width, bound_ref, shifts, rec_gain_ref, state
-        )
+                total = squares[0, k, :1]
+                for p in range(1, n):
+                    total = total + squares[p, k, :1]
+                inv_rms = lax.rsqrt(total / (feats * n) + EPS)
+                scales[...] = jnp.transpose(jnp.broadcast_to(inv_rms, (128, rows)))
+            inv_rms = scales[pl.ds(begin % rows, size)]
+            for c in range(width // 128):
+                lane = pl.ds(c * 128, 128)
+                result = part[e, span, lane] + came[e, span, lane].astype(f32)
+                x[span, lane] = (result * inv_rms).astype(bf16)
+            with scope(f"stick{u}"):
+                heads[e, span, pl.ds(0, wide)] = stick_block(
+                    begin, size, e, group, x, offset_ref
+                )
+            with scope(f"state{u}"):
+                heads[e, span, pl.ds(wide, REC_VAL)] = state_block(
+                    begin, size, x, att_width,
+                    bounds[:, pl.ds(e * REC_KEY, REC_KEY)],
+                    rec_gains[:, pl.ds(e * REC_VAL, REC_VAL)], shifts, state,
+                )
+
+        def share_copy(k, b):
+            to = lax.rem(t + b, nt)
+            return remote(
+                shares.at[k, to], landed.at[k, b], f_send.at[k, b], f_recv.at[k, b], {"tp": to}
+            )
+
+        def multiply(u):
+            begin, size = units[u]
+            k = begin // rows
+            span = pl.ds(begin, size)
+            total = None
+            for i in range(2):
+                for o, at, deep in ((0, 0, wide), (1, wide, REC_VAL)):
+                    term = dot_nn(heads[i, span, pl.ds(at, deep)], outs[o, pl.ds(i * deep, deep)])
+                    total = term if total is None else total + term
+            total = total.astype(bf16)
+            if size == rows:
+                shares[k] = total.reshape(nt, piece, cols)
+                for b in range(1, nt):
+                    share_copy(k, b).start()
+            else:
+                for j in range(begin % rows // piece, (begin % rows + size) // piece):
+                    at = j * piece - begin % rows
+                    shares[k, j] = total[at:at + piece]
+                    b = lax.rem(j - t + nt, nt)
+                    pl.when(t != j)(lambda: share_copy(k, b).start())
+
+        place = out_ref.at[:, pl.ds(v * cols, cols)]
+
+        def final_copy(k):
+            return remote(mixed.at[k], place, g_send.at[k], g_recv.at[v], {"sp": k})
+
+        def final_here():
+            return pltpu.make_async_copy(mixed.at[v], place, g_local)
+
+        def combine(k):
+            with scope(f"wshare{k}"):
+                for b in range(1, nt):
+                    share_copy(k, b).wait_recv()
+            result = shares[k, t].astype(f32)
+            for b in range(1, nt):
+                result = result + landed[k, b].astype(f32)
+            mixed[k] = result.astype(bf16)
+            if k == v:
+                final_here().start()
+            else:
+                final_copy(k).start()
+
+        def loaded(first, last):
+            for load in loads[first:last]:
+                load.wait()
+
+        events = []
+
+        def event(time, *call):
+            events.append((time, len(events), call))
+
+        starts = (START0, START1)
+        hops = (n - 1 - v, v)
+        whole = slice(None)
+        event(5.9, loaded, 1, early)
+        event(6.9, loaded, early, early + 1)
+        event(15.0, loaded, early + 1, len(loads))
+        if v == 0:
+            event(0.0, send_first)
+        for c in range(subs):
+            event(4.0 + 0.1 * c, relay, 0, c)
+        if v > 0:
+            event(4.05, send_first)
+        for c in range(subs):
+            event(6.0 + 0.1 * c, project, 0, c)
+        event(7.0, send_shift)
+        event(7.1, square, 0)
+        ready = [6.5]
+        for k in range(1, n):
+            event(6.05 if k == 1 else 9.0 + 0.1 * k, relay, k, whole)
+            at = TOKENS + TOKEN_STEP * (k - 1)
+            event(at, project, k, whole)
+            event(at + 0.1, square, k)
+            ready.append(at + 0.01)
+        chain_end = 0.0
+        if v not in ends:
+            for i in range(2):
+                for c in range(n * subs):
+                    at = max(starts[i] + hops[i] * HOP + CHUNK * c, ready[c // subs])
+                    event(at, forward, i, c)
+                    chain_end = max(chain_end, at)
+        done = [[0.0] * nu, [0.0] * nu]
         for i in range(2):
-            @pl.when(s == ends[i])
+            at = 0.0
+            for u, (begin, size) in enumerate(units):
+                last = (begin + size) // SUB - 1
+                arrive = max(at, starts[i] + (n - 1) * HOP + CHUNK * last)
+                at = arrive + (2.2 if size == rows else 1.6)
+                done[i][u] = at
+                if v == ends[i]:
+                    event(arrive, mix, u)
+                    for to in head_targets(i, u):
+                        late = 0.0
+                        if u == 0 and to == ends[1 - i]:
+                            late = 2 * CHUNK * subs
+                        event(at - 0.1 + late, send_heads, i, u, to)
+        for u, (begin, size) in enumerate(units):
+            k = begin // rows
+            latest = max(done[0][u], done[1][u])
+            for i in others:
+                if direct(u):
+                    at = done[i][u] + 5.0
+                elif v == near(i):
+                    at = done[i][u] + 4.2
+                elif v == ends[1 - i]:
+                    at = done[i][u] + 5.0 + (2 * CHUNK * subs if u == 0 else 0.0)
+                else:
+                    at = done[i][u] + 8.4
+                at = max(at, chain_end)
+                event(at, wait_heads, i, u)
+                for to in head_targets(i, u):
+                    event(at, send_heads, i, u, to)
+                latest = max(latest, at)
+            event(latest + 0.1, multiply, u)
+            if begin + size == (k + 1) * rows:
+                event(latest + 4.0, combine, k)
+        for _, _, (call, *args) in sorted(events, key=lambda e: e[:2]):
+            call(*args)
+
+        for p in range(n):
+            if p == v:
+                continue
+            with scope(f"wfinal{p}"):
+                remote(
+                    mixed.at[0], out_ref.at[:, pl.ds(p * cols, cols)], g_send.at[0], g_recv.at[p],
+                    {"sp": p},
+                ).wait_recv()
+        with scope("wlocal"):
+            final_here().wait()
+
+        with scope("wsend"):
+            for c in parts_of(v):
+                for j in range(nt):
+                    if j == v:
+                        pl.when(t != v)(lambda: first_copy(c, j).wait_send())
+                    else:
+                        first_copy(c, j).wait_send()
+            for i in others:
+                shift_copy(i).wait_send()
+            for k in range(n):
+                for d in range(1, nt):
+                    for c in parts_of(k):
+                        second_copy(k, c, d).wait_send()
+                    if k < n - 1:
+                        share_copy(k, d).wait_send()
+                    else:
+                        share_copy(k, d).wait_send()
+                for i in others:
+                    square_copy(k, i).wait_send()
+                    for r in range(subs):
+                        chain_copy(i, k * subs + r).wait_send()
+                if k != v:
+                    final_copy(k).wait_send()
+            for i in range(2):
+                for u in range(nu):
+                    for to in head_targets(i, u):
+                        head_copy(i, u, to).wait_send()
+
+    for v in range(n):
+        if v in ends:
+            @pl.when(s == v)
             def _():
-                for to in (range(n - 1, 0, -1) if i == 0 else range(n - 1)):
-                    head_copy(i, k, to).start()
-
-    def share_copy(k, b):
-        to = lax.rem(t + b, nt)
-        return remote(
-            shares.at[k, to], landed.at[k, b], f_send.at[k, b], f_recv.at[k, b], {"tp": to}
-        )
-
-    def multiply(k):
-        span = pl.ds(k * rows, rows)
-        total = None
-        for i in range(2):
-            pl.when(s != ends[i])(lambda i=i: head_copy(i, k, ends[i]).wait_recv())
-        for i in range(2):
-            for ref, first, size in ((wa_ref, 0, wide), (wr_ref, wide, REC_VAL)):
-                term = dot_nn(heads[i, span, pl.ds(first, size)], ref[pl.ds(i * size, size)])
-                total = term if total is None else total + term
-        shares[k] = total.astype(bf16).reshape(nt, piece, cols)
-        for b in range(1, nt):
-            share_copy(k, b).start()
-
-    place = out_ref.at[:, pl.ds(pl.multiple_of(s * cols, cols), cols)]
-
-    def final_copy(k):
-        return remote(mixed.at[k], place, g_send.at[k], g_recv.at[s], {"sp": k})
-
-    def final_here(k):
-        return pltpu.make_async_copy(mixed.at[k], place, g_local)
-
-    def combine(k):
-        result = shares[k, t].astype(f32)
-        for b in range(1, nt):
-            share_copy(k, b).wait_recv()
-            result = result + landed[k, b].astype(f32)
-        mixed[k] = result.astype(bf16)
-        pl.when(s != k)(lambda: final_copy(k).start())
-        pl.when(s == k)(lambda: final_here(k).start())
-
-    relay(0)
-    for k in range(n):
-        if k + 1 < n:
-            relay(k + 1)
-        project(k)
-        if k == 0:
-            for i, u in enumerate(ends):
-                pl.when(s != u)(lambda i=i: shift_copy(i).start())
-                pl.when(s == u)(lambda i=i: shift_here(i).start())
-
-    for v in range(1, n - 1):
-        events = [(c + LAG * v, 1, c) for c in range(n * subs)]
-        events += [(c + LAG * (n - 1 - v), 0, c) for c in range(n * subs)]
-
-        @pl.when(s == v)
-        def _():
-            for _, i, c in sorted(events):
-                forward(i, c)
-
-    @pl.when(at_end)
-    def _():
-        for k in range(n - 1):
-            mix(k)
-
-    multiply(0)
-
-    @pl.when(at_end)
-    def _():
-        mix(n - 1)
-
-    for k in range(1, n):
-        multiply(k)
-        combine(k - 1)
-    combine(n - 1)
-
-    for v in range(n):
-        @pl.when(s != v)
-        def _():
-            remote(
-                mixed.at[0], out_ref.at[:, pl.ds(v * cols, cols)], g_send.at[0], g_recv.at[v],
-                {"sp": v},
-            ).wait_recv()
-        pl.when(s == v)(lambda v=v: final_here(v).wait())
-
-    for j in range(nt):
-        here = (s == t) & (t == j)
-        pl.when(jnp.logical_not(here))(lambda j=j: first_copy(j).wait_send())
-    for i in range(2):
-        pl.when(s != ends[i])(lambda i=i: shift_copy(i).wait_send())
-    for k in range(n):
-        for d in range(1, nt):
-            second_copy(k, d).wait_send()
-            share_copy(k, d).wait_send()
-        for i in range(2):
-            pl.when(s != ends[i])(lambda i=i, k=k: square_copy(k, i).wait_send())
-
-            @pl.when(s == ends[i])
-            def _():
-                for to in range(n):
-                    if to != ends[i]:
-                        head_copy(i, k, to).wait_send()
-
-            @pl.when(s != ends[i])
-            def _():
-                for r in range(subs):
-                    chain_copy(i, k * subs + r).wait_send()
-        pl.when(s != k)(lambda k=k: final_copy(k).wait_send())
+                x[pl.ds((n - 1) * rows, rows)] = jnp.zeros((rows, width), bf16)
+                plane(v)
+        else:
+            pl.when(s == v)(functools.partial(plane, v))
+
+
+START0, START1, HOP, CHUNK = 8.0, 6.0, 3.4, 0.88
+TOKENS, TOKEN_STEP = 10.5, 1.0
 
 
 def stationary_fits(args):
@@ -641,6 +803,8 @@
         and (att_q.shape[0] // att_k.shape[0]) * HEAD == 128
         and feats == att_q.shape[1]
         and rows == 128
+        and rows == SUB * nt
+        and SUB == ROWS8 * nt
     )
 
 
@@ -650,25 +814,36 @@
     score_offset, lower_bound, decay_shift, rec_gain = args[10:]
     rows, feats = tokens.shape
     seq = rows * n
-    cols = args[8].shape[1]
+    deep, cols = args[8].shape
     group = att_q.shape[0] // att_k.shape[0]
     width = (group + 2) * HEAD + 2 * REC_KEY + REC_VAL
     wide = group * HEAD + REC_VAL
     piece = rows // nt
     chunks = seq // SUB
+    subs = rows // SUB
+    nu = len(units_of(n, rows))
     bf16, f32 = jnp.bfloat16, jnp.float32
     dma = pltpu.SemaphoreType.DMA
     vmem = pl.BlockSpec(memory_space=pltpu.VMEM)
+    hbm = pl.BlockSpec(memory_space=pl.ANY)
     smem = pl.BlockSpec(memory_space=pltpu.SMEM)
     return pl.pallas_call(
         functools.partial(layer_kernel, n, nt, group),
         out_shape=jax.ShapeDtypeStruct((piece, cols * n), bf16),
-        in_specs=[vmem] * 11 + [smem, vmem, vmem],
-        out_specs=vmem,
+        in_specs=[hbm] * 11 + [smem, hbm, hbm],
+        out_specs=hbm,
         scratch_shapes=[
-            pltpu.VMEM((n, nt, piece, feats), bf16),
+            pltpu.VMEM((subs, nt, ROWS8, feats), bf16),
+            pltpu.VMEM((1, feats), f32),
+            pltpu.VMEM((1, 2 * REC_KEY), f32),
+            pltpu.VMEM((1, 2 * REC_VAL), f32),
+            pltpu.VMEM((2, width, feats), bf16),
+            pltpu.VMEM((2, deep, cols), bf16),
+            pltpu.VMEM((rows, 2 * REC_KEY), f32),
+            pltpu.VMEM((n, subs, nt, ROWS8, feats), bf16),
             pltpu.VMEM((seq, REC_KEY), f32),
             pltpu.VMEM((n, n, 8, rows), f32),
+            pltpu.VMEM((rows, 128), f32),
             pltpu.VMEM((2, seq, width), f32),
             pltpu.VMEM((2, seq, width), bf16),
             pltpu.VMEM((2, seq, width), bf16),
@@ -678,14 +853,17 @@
             pltpu.VMEM((n, nt, piece, cols), bf16),
             pltpu.VMEM((n, nt, piece, cols), bf16),
             pltpu.VMEM((n, piece, cols), bf16),
-            dma((nt,)), dma((n,)), dma, dma((n, nt)), dma((n, nt)), dma((2,)), dma((n,)), dma,
+            dma((19,)),
+            dma((subs, nt)), dma((n, subs)), dma((subs,)),
+            dma((n, subs, nt)), dma((n, subs, nt)), dma((2,)), dma((n,)), dma,
             dma((n, 2)), dma((n, n)), dma((2, chunks)), dma((2, chunks)),
-            dma((n, n)), dma((2, n)), dma((n, nt)), dma((n, nt)), dma((n,)), dma((n,)), dma,
+            dma((nu, n)), dma((2, nu)), dma((n, nt)), dma((n, nt)), dma((n,)), dma((n,)), dma,
         ],
         compiler_params=pltpu.CompilerParams(collective_id=0, has_side_effects=True),
         name="layer",
     )(
-        tokens, norm_gain.reshape(1, -1), *args[2:8], decay_shift, args[8], args[9],
+        tokens.reshape(subs, nt, ROWS8, feats), norm_gain.reshape(1, -1), *args[2:8], decay_shift,
+        args[8], args[9],
         score_offset, lower_bound.reshape(1, -1), rec_gain.reshape(1, -1),
     )
 

time: 64.7 us -> 59.8 us (0.924)
  Pallas kernels: 62.5 us -> 58.1 us
    pallas_call x1, Pallas kernels: 62.5 us -> 58.1 us  [stationary(): pl.pallas_call(functools.partial(layer_kernel, n, nt, group), out_shape=j...]
where the time goes in v1:
time: 59.8 us; the launch traced here: 59.6 us
  Pallas kernels  58.1 us (97%)
  local copies, waits for them, and re-layouts  1.57 us (3%)
    pallas_call x1, Pallas kernels, stationary(): pl.pallas_call(functools.partial(layer_kernel, n, nt, group), out_shape=j...  58.1 us
    unnamed x1, local copies, waits for them, and re-layouts  1.57 us

profile of v1, /device:TPU:0, one launch (start us, length us, event | category | flops | bytes accessed | tf_op | source)
XLA Modules:
  0.0 59.6 jit_solution(8996781516521685623)
XLA Ops:
  0.0 58.1 %layer.1 = bf16[32,2048]{1,0:T(8,128)(2,1)} custom-call(bf16[4,4,8,512]{3,2,1,0:T(8,128)(2,1)} %bitcast.4, f32[1,2048]{1,0:T(1,128)} %bitcast.5, bf16[256,512]{1,0:T(8,128)(2,1)} %aq_ref.1, bf16[128,512]{1,0:T(8,128)(2,1)} %ak_ref.1, bf16[128,512]{1,0:T(8,128)(2,1)} %av_ref.1, bf16[256,512]{1,0:T(8,128)(2,1)} %rq_ref.1, bf16[256,512]{1,0:T(8,128)(2,1)} %rf_ref.1, ...), custom_call_target="tpu_custom_call" | custom-call | tf_op jit(solution)/shard_map/layer/pallas_call | solution.py:830
  58.1 1.6 %copy.16 = bf16[32,2048]{1,0:T(8,128)(2,1)} copy(bf16[32,2048]{1,0:T(8,128)(2,1)} %layer.1) | data formatting | bytes 262144

commit v2 on v1

--- a/solution.py
+++ b/solution.py
@@ -323,7 +323,7 @@
     query = x[at, first:first + REC_KEY].astype(jnp.float32)
     logit = x[at, first + REC_KEY:first + 2 * REC_KEY].astype(jnp.float32)
     value = x[at, first + 2 * REC_KEY:first + 2 * REC_KEY + REC_VAL]
-    log_decay = jnp.log(bound + gap * jax.nn.sigmoid(logit)) + shift_ref[at]
+    log_decay = jnp.log(bound + gap * jax.nn.sigmoid(logit)) + shift_ref[at].astype(jnp.float32)
     keyed = gap * jax.nn.sigmoid(-logit)
     query = query * jax.nn.sigmoid(query)
     running = jnp.dot(upto, log_decay, precision=TOP_PRECISION, preferred_element_type=jnp.float32)
@@ -360,10 +360,10 @@
     tok_ref, gain_ref, aq_ref, ak_ref, av_ref, rq_ref, rf_ref, ri_ref, shift_ref,
     wa_ref, wr_ref, offset_ref, bound_ref, rec_gain_ref,
     out_ref,
-    tokens, gains, bounds, rec_gains, weights, outs, own_shift, tbuf, shifts, squares, scales,
+    tokens, gains, bounds, rec_gains, weights, outs, wide_shift, own_shift, tbuf, shifts, squares, scales,
     part, sent, came, x, state, heads, shares, landed, mixed,
-    l_sem, a_send, a_recv, a_local, b_send, b_recv, d_send, d_recv, d_local, q_send, q_recv,
-    c_send, c_recv, e_send, e_recv, f_send, f_recv, g_send, g_recv, g_local,
+    l_sem, a_send, a_recv, b_send, b_recv, d_send, d_recv, q_send, q_recv,
+    c_send, c_recv, e_send, e_recv, f_send, f_recv, g_send, g_recv,
 ):
     s, t = lax.axis_index("sp"), lax.axis_index("tp")
     rows, feats = own_shift.shape[0], tokens.shape[-1]
@@ -378,33 +378,31 @@
     units = units_of(n, rows)
     nu = len(units)
 
-    loads = [
-        pltpu.make_async_copy(tok_ref, tokens, l_sem.at[0]),
-        pltpu.make_async_copy(
-            gain_ref.at[:, pl.ds(pl.multiple_of(s * feats, feats), feats)], gains, l_sem.at[1]
-        ),
-    ]
+    load_tokens = pltpu.make_async_copy(tok_ref, tokens, l_sem.at[0])
+    load_gain = pltpu.make_async_copy(
+        gain_ref.at[:, pl.ds(pl.multiple_of(s * feats, feats), feats)], gains, l_sem.at[1]
+    )
+    load_weights = []
     first = 0
     for ref, size in (
         (aq_ref, wide), (ak_ref, HEAD), (av_ref, HEAD),
         (rq_ref, REC_KEY), (rf_ref, REC_KEY), (ri_ref, REC_VAL),
     ):
         for i in range(2):
-            loads.append(
+            load_weights.append(
                 pltpu.make_async_copy(
-                    ref.at[pl.ds(i * size, size)], weights.at[i, pl.ds(first, size)],
-                    l_sem.at[len(loads)],
+                    ref.at[pl.ds(i * size, size)], weights.at[i, pl.ds(first, size)], l_sem.at[2]
                 )
             )
         first += size
-    early = len(loads)
-    loads.append(pltpu.make_async_copy(shift_ref, own_shift, l_sem.at[early]))
-    loads.append(pltpu.make_async_copy(bound_ref, bounds, l_sem.at[early + 1]))
-    loads.append(pltpu.make_async_copy(rec_gain_ref, rec_gains, l_sem.at[early + 2]))
-    loads.append(pltpu.make_async_copy(wa_ref, outs.at[0], l_sem.at[early + 3]))
-    loads.append(pltpu.make_async_copy(wr_ref, outs.at[1], l_sem.at[early + 4]))
-
-    loads[0].start()
+    load_shift = pltpu.make_async_copy(shift_ref, wide_shift, l_sem.at[3])
+    load_bounds = pltpu.make_async_copy(bound_ref, bounds, l_sem.at[4])
+    load_rec_gains = pltpu.make_async_copy(rec_gain_ref, rec_gains, l_sem.at[5])
+    load_outs = [
+        pltpu.make_async_copy(ref, outs.at[o], l_sem.at[6]) for o, ref in enumerate((wa_ref, wr_ref))
+    ]
+
+    load_tokens.start()
     barrier = pltpu.get_barrier_semaphore()
     for a in range(n):
         for b in range(nt):
@@ -414,9 +412,11 @@
                     device_id={"sp": lax.rem(s + a, n), "tp": lax.rem(t + b, nt)},
                     device_id_type=MESH,
                 )
-    for load in loads[1:]:
+    for load in (
+        load_shift, load_gain, *load_weights, load_bounds, load_rec_gains, *load_outs
+    ):
         load.start()
-    loads[0].wait()
+    load_tokens.wait()
     with scope("barrier"):
         pl.semaphore_wait(barrier, n * nt - 1)
 
@@ -431,18 +431,24 @@
         def slot(c):
             return 0 if isinstance(c, slice) else c
 
+        def lane_of(k, c):
+            return c if k == 0 else subs + k - 1
+
         def first_copy(c, j):
             return remote(
-                tokens.at[c, j], tbuf.at[v, c, j], a_send.at[slot(c), j], a_recv.at[v, slot(c)],
+                tokens.at[c, j], tbuf.at[v, c, j], a_send, a_recv.at[lane_of(v, c)],
                 {"sp": t, "tp": j},
             )
 
         def first_here(c):
             return pltpu.make_async_copy(
-                tokens.at[c, v], tbuf.at[v, c, v], a_local.at[slot(c)]
-            )
-
-        def send_first():
+                tokens.at[c, v], tbuf.at[v, c, v], a_recv.at[lane_of(v, c)]
+            )
+
+        def send_first(when):
+            pl.when(when)(send_first_now)
+
+        def send_first_now():
             for c in parts_of(v):
                 for j in range(nt):
                     if j == v:
@@ -454,29 +460,22 @@
         def second_copy(k, c, d):
             return remote(
                 tbuf.at[k, c, t], tbuf.at[k, c, t],
-                b_send.at[k, slot(c), d], b_recv.at[k, slot(c), d],
+                b_send, b_recv.at[lane_of(k, c)],
                 {"tp": lax.rem(t + d, nt)},
             )
 
         def relay(k, c):
-            def arrived():
+            with scope(f"relay{k}"):
                 remote(
-                    tokens.at[c, 0], tbuf.at[k, c, t], a_send.at[0, 0], a_recv.at[k, slot(c)],
+                    tokens.at[c, 0], tbuf.at[k, c, t], a_send, a_recv.at[lane_of(k, c)],
                     {"sp": (v + 1) % n},
                 ).wait_recv()
-
-            with scope(f"relay{k}"):
-                if k == v:
-                    pl.when(t != v)(arrived)
-                    pl.when(t == v)(lambda: first_here(c).wait())
-                else:
-                    arrived()
             for d in range(1, nt):
                 second_copy(k, c, d).start()
 
         def square_copy(k, i):
             return remote(
-                squares.at[v, k], squares.at[v, k], q_send.at[k, i], q_recv.at[v, k],
+                squares.at[v, k], squares.at[v, k], q_send.at[i], q_recv.at[k],
                 {"sp": ends[i]},
             )
 
@@ -484,13 +483,15 @@
             to = v - 1 if i == 0 else v + 1
             return remote(
                 sent.at[i, pl.ds(c * SUB, SUB)], came.at[i, pl.ds(c * SUB, SUB)],
-                c_send.at[i, c], c_recv.at[i, c], {"sp": to},
+                c_send.at[i], c_recv.at[i, c], {"sp": to},
             )
 
         def project(k, c):
             with scope(f"wtok{k}"):
-                for d in range(1, nt):
-                    second_copy(k, c, d).wait_recv()
+                most = tbuf.at[k, c, pl.ds(0, nt - 1)]
+                remote(
+                    most, most, b_send, b_recv.at[lane_of(k, c)], {"tp": lax.rem(t + 1, nt)}
+                ).wait_recv()
             size = rows if isinstance(c, slice) else SUB
             begin = k * rows + slot(c) * SUB
             raw = tbuf[k, c].reshape(size, feats).astype(f32)
@@ -522,14 +523,14 @@
         def shift_here(i):
             return pltpu.make_async_copy(
                 own_shift.at[:, pl.ds(i * REC_KEY, REC_KEY)], shifts.at[pl.ds(v * rows, rows)],
-                d_local,
-            )
-
-        def send_shift():
-            for i in others:
+                d_recv.at[v],
+            )
+
+        def send_shift(i):
+            if v == ends[i]:
+                shift_here(i).start()
+            else:
                 shift_copy(i).start()
-            for i in mine:
-                shift_here(i).start()
 
         def forward(i, c):
             with scope(f"chain{i}_{c}"):
@@ -541,7 +542,7 @@
         def head_copy(i, u, to):
             at = (i, pl.ds(units[u][0], units[u][1]))
             return remote(
-                heads.at[at], heads.at[at], e_send.at[u, to], e_recv.at[i, u], {"sp": to}
+                heads.at[at], heads.at[at], e_send.at[to], e_recv.at[i, u], {"sp": to}
             )
 
         def near(i):
@@ -553,12 +554,17 @@
         def direct(u):
             return units[u][1] == LAST
 
+        def relayed(i, u):
+            return u == 0 or (u == 1 and i == 1)
+
         def head_targets(i, u):
+            far = ends[1 - i]
+            if relayed(i, u):
+                return [] if v == far else [v + 1 if i == 0 else v - 1]
             if v == ends[i]:
-                far = ends[1 - i]
                 if direct(u):
                     return [far, *between(i), near(i)]
-                return [far, near(i)]
+                return [near(i), far]
             if v == near(i) and not direct(u):
                 return between(i)
             return []
@@ -579,19 +585,13 @@
                 for c in range(begin // SUB, (begin + size) // SUB):
                     chain_copy(e, c).wait_recv()
             if begin % rows == 0:
-                for p in range(n):
-                    if p != v:
-                        remote(
-                            squares.at[p, k], squares.at[p, k], q_send.at[k, e], q_recv.at[p, k],
-                            {"sp": p},
-                        ).wait_recv()
-                if k == v:
-                    shift_here(e).wait()
-                else:
-                    remote(
-                        own_shift.at[:, pl.ds(e * REC_KEY, REC_KEY)],
-                        shifts.at[pl.ds(k * rows, rows)], d_send.at[e], d_recv.at[k], {"sp": k},
-                    ).wait_recv()
+                most = squares.at[pl.ds(0, n - 1), k]
+                remote(most, most, q_send.at[e], q_recv.at[k], {"sp": ends[1 - e]}).wait_recv()
+                remote(
+                    own_shift.at[:, pl.ds(e * REC_KEY, REC_KEY)],
+                    shifts.at[pl.ds(k * rows, rows)], d_send.at[e], d_recv.at[k],
+                    {"sp": ends[1 - e]},
+                ).wait_recv()
                 total = squares[0, k, :1]
                 for p in range(1, n):
                     total = total + squares[p, k, :1]
@@ -616,7 +616,7 @@
         def share_copy(k, b):
             to = lax.rem(t + b, nt)
             return remote(
-                shares.at[k, to], landed.at[k, b], f_send.at[k, b], f_recv.at[k, b], {"tp": to}
+                shares.at[k, to], landed.at[k, b], f_send, f_recv.at[k], {"tp": to}
             )
 
         def multiply(u):
@@ -643,15 +643,18 @@
         place = out_ref.at[:, pl.ds(v * cols, cols)]
 
         def final_copy(k):
-            return remote(mixed.at[k], place, g_send.at[k], g_recv.at[v], {"sp": k})
+            return remote(mixed.at[k], place, g_send, g_recv, {"sp": k})
 
         def final_here():
-            return pltpu.make_async_copy(mixed.at[v], place, g_local)
+            return pltpu.make_async_copy(mixed.at[v], place, g_recv)
 
         def combine(k):
             with scope(f"wshare{k}"):
-                for b in range(1, nt):
-                    share_copy(k, b).wait_recv()
+                most = pl.ds(1, nt - 1)
+                remote(
+                    shares.at[k, most], landed.at[k, most], f_send, f_recv.at[k],
+                    {"tp": lax.rem(t + 1, nt)},
+                ).wait_recv()
             result = shares[k, t].astype(f32)
             for b in range(1, nt):
                 result = result + landed[k, b].astype(f32)
@@ -661,9 +664,14 @@
             else:
                 final_copy(k).start()
 
-        def loaded(first, last):
-            for load in loads[first:last]:
-                load.wait()
+        def projection_loaded():
+            load_gain.wait()
+            pltpu.make_async_copy(weights, weights, l_sem.at[2]).wait()
+
+        def rest_loaded():
+            load_bounds.wait()
+            load_rec_gains.wait()
+            pltpu.make_async_copy(outs, outs, l_sem.at[6]).wait()
 
         events = []
 
@@ -673,23 +681,31 @@
         starts = (START0, START1)
         hops = (n - 1 - v, v)
         whole = slice(None)
-        event(5.9, loaded, 1, early)
-        event(6.9, loaded, early, early + 1)
-        event(15.0, loaded, early + 1, len(loads))
+        event(5.9, projection_loaded)
+        def round_shift():
+            own_shift[...] = wide_shift[...].astype(bf16)
+
+        event(0.1, load_shift.wait)
+        event(0.15, round_shift)
+        event(15.0, rest_loaded)
+        soon = t < v
+        if v < n // 2:
+            soon = soon | (t == n - 1)
         if v == 0:
-            event(0.0, send_first)
+            soon = t >= 0
+        event(0.0, send_first, soon)
         for c in range(subs):
             event(4.0 + 0.1 * c, relay, 0, c)
-        if v > 0:
-            event(4.05, send_first)
+        event(4.05, send_first, jnp.logical_not(soon))
         for c in range(subs):
             event(6.0 + 0.1 * c, project, 0, c)
-        event(7.0, send_shift)
+        event(0.2, send_shift, 0)
+        event(4.4 if 0 < v < n - 1 else 0.2, send_shift, 1)
         event(7.1, square, 0)
         ready = [6.5]
         for k in range(1, n):
             event(6.05 if k == 1 else 9.0 + 0.1 * k, relay, k, whole)
-            at = TOKENS + TOKEN_STEP * (k - 1)
+            at = (TOKENS if v in ends else TOKENS_MID)[k - 1]
             event(at, project, k, whole)
             event(at + 0.1, square, k)
             ready.append(at + 0.01)
@@ -706,28 +722,30 @@
             for u, (begin, size) in enumerate(units):
                 last = (begin + size) // SUB - 1
                 arrive = max(at, starts[i] + (n - 1) * HOP + CHUNK * last)
-                at = arrive + (2.2 if size == rows else 1.6)
+                at = arrive + (1.8 if size == rows else 1.6)
                 done[i][u] = at
                 if v == ends[i]:
                     event(arrive, mix, u)
                     for to in head_targets(i, u):
-                        late = 0.0
-                        if u == 0 and to == ends[1 - i]:
-                            late = 2 * CHUNK * subs
-                        event(at - 0.1 + late, send_heads, i, u, to)
+                        event(at - 0.1, send_heads, i, u, to)
         for u, (begin, size) in enumerate(units):
             k = begin // rows
             latest = max(done[0][u], done[1][u])
             for i in others:
+                away = v if i == 0 else n - 1 - v
                 if direct(u):
                     at = done[i][u] + 5.0
+                elif relayed(i, u):
+                    at = done[i][u] + 4.2 * away
                 elif v == near(i):
                     at = done[i][u] + 4.2
                 elif v == ends[1 - i]:
-                    at = done[i][u] + 5.0 + (2 * CHUNK * subs if u == 0 else 0.0)
+                    at = done[i][u] + 6.5
                 else:
                     at = done[i][u] + 8.4
-                at = max(at, chain_end)
+                latest = max(latest, chain_end)
+                if v != near(i):
+                    at = max(at, chain_end)
                 event(at, wait_heads, i, u)
                 for to in head_targets(i, u):
                     event(at, send_heads, i, u, to)
@@ -738,44 +756,30 @@
         for _, _, (call, *args) in sorted(events, key=lambda e: e[:2]):
             call(*args)
 
-        for p in range(n):
-            if p == v:
-                continue
-            with scope(f"wfinal{p}"):
-                remote(
-                    mixed.at[0], out_ref.at[:, pl.ds(p * cols, cols)], g_send.at[0], g_recv.at[p],
-                    {"sp": p},
-                ).wait_recv()
-        with scope("wlocal"):
-            final_here().wait()
+        with scope("wfinal"):
+            pltpu.make_async_copy(out_ref, out_ref, g_recv).wait()
 
         with scope("wsend"):
-            for c in parts_of(v):
-                for j in range(nt):
-                    if j == v:
-                        pl.when(t != v)(lambda: first_copy(c, j).wait_send())
-                    else:
-                        first_copy(c, j).wait_send()
+            def sent_all(src, sem):
+                remote(src, src, sem, a_recv.at[0], {"sp": (v + 1) % n}).wait_send()
+
+            pl.when(t != v)(lambda: sent_all(tokens, a_send))
+            pl.when(t == v)(lambda: sent_all(tokens.at[:, pl.ds(0, nt - 1)], a_send))
+            sent_all(tbuf.at[:, :, pl.ds(0, nt - 1)], b_send)
+            sent_all(shares.at[:, pl.ds(0, nt - 1)], f_send)
+            sent_all(mixed.at[pl.ds(0, n - 1)], g_send)
             for i in others:
-                shift_copy(i).wait_send()
-            for k in range(n):
-                for d in range(1, nt):
-                    for c in parts_of(k):
-                        second_copy(k, c, d).wait_send()
-                    if k < n - 1:
-                        share_copy(k, d).wait_send()
-                    else:
-                        share_copy(k, d).wait_send()
-                for i in others:
-                    square_copy(k, i).wait_send()
-                    for r in range(subs):
-                        chain_copy(i, k * subs + r).wait_send()
-                if k != v:
-                    final_copy(k).wait_send()
-            for i in range(2):
-                for u in range(nu):
-                    for to in head_targets(i, u):
-                        head_copy(i, u, to).wait_send()
+                sent_all(own_shift.at[:, pl.ds(i * REC_KEY, REC_KEY)], d_send.at[i])
+                sent_all(squares.at[v], q_send.at[i])
+                sent_all(sent.at[i], c_send.at[i])
+            for to in range(n):
+                spans = [
+                    units[u] for i in range(2) for u in range(nu) if to in head_targets(i, u)
+                ]
+                if spans:
+                    begin = spans[0][0]
+                    size = sum(size for _, size in spans)
+                    sent_all(heads.at[0, pl.ds(begin, size)], e_send.at[to])
 
     for v in range(n):
         if v in ends:
@@ -787,8 +791,9 @@
             pl.when(s == v)(functools.partial(plane, v))
 
 
-START0, START1, HOP, CHUNK = 8.0, 6.0, 3.4, 0.88
-TOKENS, TOKEN_STEP = 10.5, 1.0
+START0, START1, HOP, CHUNK = 8.0, 6.3, 3.6, 0.88
+TOKENS = (10.5, 11.5, 12.5)
+TOKENS_MID = (10.5, 14.0, 16.5)
 
 
 def stationary_fits(args):
@@ -840,8 +845,9 @@
             pltpu.VMEM((2, width, feats), bf16),
             pltpu.VMEM((2, deep, cols), bf16),
             pltpu.VMEM((rows, 2 * REC_KEY), f32),
+            pltpu.VMEM((rows, 2 * REC_KEY), bf16),
             pltpu.VMEM((n, subs, nt, ROWS8, feats), bf16),
-            pltpu.VMEM((seq, REC_KEY), f32),
+            pltpu.VMEM((seq, REC_KEY), bf16),
             pltpu.VMEM((n, n, 8, rows), f32),
             pltpu.VMEM((rows, 128), f32),
             pltpu.VMEM((2, seq, width), f32),
@@ -853,11 +859,9 @@
             pltpu.VMEM((n, nt, piece, cols), bf16),
             pltpu.VMEM((n, nt, piece, cols), bf16),
             pltpu.VMEM((n, piece, cols), bf16),
-            dma((19,)),
-            dma((subs, nt)), dma((n, subs)), dma((subs,)),
-            dma((n, subs, nt)), dma((n, subs, nt)), dma((2,)), dma((n,)), dma,
-            dma((n, 2)), dma((n, n)), dma((2, chunks)), dma((2, chunks)),
-            dma((nu, n)), dma((2, nu)), dma((n, nt)), dma((n, nt)), dma((n,)), dma((n,)), dma,
+            dma((7,)), dma, dma((subs + n - 1,)), dma, dma((subs + n - 1,)), dma((2,)), dma((n,)),
+            dma((2,)), dma((n,)), dma((2,)), dma((2, chunks)), dma((n,)), dma((2, nu)),
+            dma, dma((n,)), dma, dma,
         ],
         compiler_params=pltpu.CompilerParams(collective_id=0, has_side_effects=True),
         name="layer",

time: 59.8 us -> 52.3 us (0.87)
  Pallas kernels: 58.1 us -> 50.6 us
    pallas_call x1, Pallas kernels: 58.1 us -> 50.6 us  [stationary(): pl.pallas_call(functools.partial(layer_kernel, n, nt, group), out_shape=j...]
where the time goes in v2:
time: 52.3 us; the launch traced here: 52.2 us
  Pallas kernels  50.6 us (97%)
  local copies, waits for them, and re-layouts  1.57 us (3%)
    pallas_call x1, Pallas kernels, stationary(): pl.pallas_call(functools.partial(layer_kernel, n, nt, group), out_shape=j...  50.6 us
    unnamed x1, local copies, waits for them, and re-layouts  1.57 us

profile of v2, /device:TPU:0, one launch (start us, length us, event | category | flops | bytes accessed | tf_op | source)
XLA Modules:
  0.0 52.2 jit_solution(5945216065053252391)
XLA Ops:
  0.0 50.6 %layer.1 = bf16[32,2048]{1,0:T(8,128)(2,1)} custom-call(bf16[4,4,8,512]{3,2,1,0:T(8,128)(2,1)} %bitcast.4, f32[1,2048]{1,0:T(1,128)} %bitcast.5, bf16[256,512]{1,0:T(8,128)(2,1)} %aq_ref.1, bf16[128,512]{1,0:T(8,128)(2,1)} %ak_ref.1, bf16[128,512]{1,0:T(8,128)(2,1)} %av_ref.1, bf16[256,512]{1,0:T(8,128)(2,1)} %rq_ref.1, bf16[256,512]{1,0:T(8,128)(2,1)} %rf_ref.1, ...), custom_call_target="tpu_custom_call" | custom-call | tf_op jit(solution)/shard_map/layer/pallas_call | solution.py:835
  50.6 1.6 %copy.16 = bf16[32,2048]{1,0:T(8,128)(2,1)} copy(bf16[32,2048]{1,0:T(8,128)(2,1)} %layer.1) | data formatting | bytes 262144

commit v3 on v2

--- a/solution.py
+++ b/solution.py
@@ -292,7 +292,7 @@
         keys = x[c * block:(c + 1) * block, group * HEAD:(group + 1) * HEAD]
         values = x[c * block:(c + 1) * block, (group + 1) * HEAD:(group + 2) * HEAD]
         score = dot_nt(queries, keys) * HEAD ** (-0.5) + offset
-        keep = -(jnp.maximum(score, 0.0) + jnp.log1p(jnp.exp(-jnp.abs(score))))
+        keep = -(jnp.maximum(score, 0.0) + jnp.log(1.0 + jnp.exp(-jnp.abs(score))))
         gate = score + keep
         if c == q:
             keep = jnp.where(visible, keep, 0.0)
@@ -351,8 +351,9 @@
 
 
 def units_of(n, rows):
-    whole = [(k * rows, rows) for k in range(n - 1)]
-    return whole + [((n - 1) * rows + r, LAST) for r in range(0, rows, LAST)]
+    seq = n * rows
+    whole = [(k * rows, rows) for k in range(n - 2)]
+    return whole + [(r, LAST) for r in range((n - 2) * rows, seq, LAST)]
 
 
 def layer_kernel(
@@ -551,21 +552,21 @@
         def between(i):
             return [p for p in range(1, n - 1) if p != near(i)]
 
-        def direct(u):
-            return units[u][1] == LAST
+        def direct(i, u):
+            return MODES[i][units[u][0] // rows] == 2
 
         def relayed(i, u):
-            return u == 0 or (u == 1 and i == 1)
+            return MODES[i][units[u][0] // rows] == 0
 
         def head_targets(i, u):
             far = ends[1 - i]
             if relayed(i, u):
                 return [] if v == far else [v + 1 if i == 0 else v - 1]
             if v == ends[i]:
-                if direct(u):
+                if direct(i, u):
                     return [far, *between(i), near(i)]
                 return [near(i), far]
-            if v == near(i) and not direct(u):
+            if v == near(i) and not direct(i, u):
                 return between(i)
             return []
 
@@ -716,43 +717,52 @@
                     at = max(starts[i] + hops[i] * HOP + CHUNK * c, ready[c // subs])
                     event(at, forward, i, c)
                     chain_end = max(chain_end, at)
+        def distance(i, p):
+            return p if i == 0 else n - 1 - p
+
+        def leaves(i, u, to):
+            last = starts[1 - i] + distance(i, to) * HOP + CHUNK * (n * subs - 1)
+            return max(done[i][u] - 0.1, last - FAR)
+
         done = [[0.0] * nu, [0.0] * nu]
         for i in range(2):
             at = 0.0
             for u, (begin, size) in enumerate(units):
                 last = (begin + size) // SUB - 1
                 arrive = max(at, starts[i] + (n - 1) * HOP + CHUNK * last)
-                at = arrive + (1.8 if size == rows else 1.6)
+                at = arrive + (1.8 if size == rows else 1.45)
                 done[i][u] = at
                 if v == ends[i]:
                     event(arrive, mix, u)
                     for to in head_targets(i, u):
-                        event(at - 0.1, send_heads, i, u, to)
+                        event(leaves(i, u, to), send_heads, i, u, to)
         for u, (begin, size) in enumerate(units):
             k = begin // rows
-            latest = max(done[0][u], done[1][u])
+            latest = max(done[0][u], done[1][u], chain_end + 0.01)
             for i in others:
-                away = v if i == 0 else n - 1 - v
-                if direct(u):
-                    at = done[i][u] + 5.0
-                elif relayed(i, u):
-                    at = done[i][u] + 4.2 * away
-                elif v == near(i):
-                    at = done[i][u] + 4.2
-                elif v == ends[1 - i]:
-                    at = done[i][u] + 6.5
+                load = 1.4 * size / rows
+                away = distance(i, v)
+                if relayed(i, u):
+                    at = leaves(i, u, near(i)) + (3.0 + load) * away
+                elif direct(i, u):
+                    at = leaves(i, u, v) + 2.8 + 0.45 * away + (n - away) * load
+                elif v in between(i):
+                    at = leaves(i, u, near(i)) + 6.5 + 2 * load
                 else:
-                    at = done[i][u] + 8.4
-                latest = max(latest, chain_end)
-                if v != near(i):
-                    at = max(at, chain_end)
+                    at = leaves(i, u, v) + 2.8 + 0.45 * away + load
+                if v in ends:
+                    at = max(at, done[mine[0]][nu - 1] + 0.01)
+                elif v == 1 and i == 0 and relayed(i, u):
+                    at -= 0.2
+                else:
+                    at = max(at, chain_end + 0.01)
                 event(at, wait_heads, i, u)
                 for to in head_targets(i, u):
                     event(at, send_heads, i, u, to)
                 latest = max(latest, at)
-            event(latest + 0.1, multiply, u)
+            event(latest + 0.02, multiply, u)
             if begin + size == (k + 1) * rows:
-                event(latest + 4.0, combine, k)
+                event(latest + 4.5, combine, k)
         for _, _, (call, *args) in sorted(events, key=lambda e: e[:2]):
             call(*args)
 
@@ -785,13 +795,15 @@
         if v in ends:
             @pl.when(s == v)
             def _():
-                x[pl.ds((n - 1) * rows, rows)] = jnp.zeros((rows, width), bf16)
+                x[...] = jnp.zeros_like(x)
                 plane(v)
         else:
             pl.when(s == v)(functools.partial(plane, v))
 
 
 START0, START1, HOP, CHUNK = 8.0, 6.3, 3.6, 0.88
+FAR = 3.2
+MODES = ((0, 1, 1, 1), (0, 0, 1, 1))
 TOKENS = (10.5, 11.5, 12.5)
 TOKENS_MID = (10.5, 14.0, 16.5)
 
@@ -834,9 +846,9 @@
     smem = pl.BlockSpec(memory_space=pltpu.SMEM)
     return pl.pallas_call(
         functools.partial(layer_kernel, n, nt, group),
-        out_shape=jax.ShapeDtypeStruct((piece, cols * n), bf16),
+        out_shape=pltpu.VMEM((piece, cols * n), bf16),
         in_specs=[hbm] * 11 + [smem, hbm, hbm],
-        out_specs=hbm,
+        out_specs=vmem,
         scratch_shapes=[
             pltpu.VMEM((subs, nt, ROWS8, feats), bf16),
             pltpu.VMEM((1, feats), f32),

time: 52.3 us -> 51 us (0.975)
  local copies, waits for them, and re-layouts: 1.57 us -> 0.66 us
    unnamed x1, local copies, waits for them, and re-layouts: 1.57 us -> 0.66 us
where the time goes in v3:
time: 51 us; the launch traced here: 50.9 us
  Pallas kernels  50.2 us (98%)
  local copies, waits for them, and re-layouts  0.66 us (1%)
    pallas_call x1, Pallas kernels, stationary(): pl.pallas_call(functools.partial(layer_kernel, n, nt, group), out_shape=p...  50.2 us

profile of v3, /device:TPU:0, one launch (start us, length us, event | category | flops | bytes accessed | tf_op | source)
XLA Modules:
  0.0 50.9 jit_solution(18054223588034001484)
XLA Ops:
  0.0 50.2 %layer.1 = bf16[32,2048]{1,0:T(8,128)(2,1)S(1)} custom-call(bf16[4,4,8,512]{3,2,1,0:T(8,128)(2,1)} %bitcast.4, f32[1,2048]{1,0:T(1,128)} %bitcast.5, bf16[256,512]{1,0:T(8,128)(2,1)} %aq_ref.1, bf16[128,512]{1,0:T(8,128)(2,1)} %ak_ref.1, bf16[128,512]{1,0:T(8,128)(2,1)} %av_ref.1, bf16[256,512]{1,0:T(8,128)(2,1)} %rq_ref.1, bf16[256,512]{1,0:T(8,128)(2,1)} %rf_ref.1, ...), custom_call_target="tpu_custom_call" | custom-call | tf_op jit(solution)/shard_map/layer/pallas_call | solution.py:847
  50.2 0.7 %copy.16 = bf16[32,2048]{1,0:T(8,128)(2,1)} copy(bf16[32,2048]{1,0:T(8,128)(2,1)S(1)} %layer.1) | data formatting | bytes 262144

commit v4 on v3

--- a/solution.py
+++ b/solution.py
@@ -762,7 +762,7 @@
                 latest = max(latest, at)
             event(latest + 0.02, multiply, u)
             if begin + size == (k + 1) * rows:
-                event(latest + 4.5, combine, k)
+                event(latest + 6.0, combine, k)
         for _, _, (call, *args) in sorted(events, key=lambda e: e[:2]):
             call(*args)
 
@@ -801,7 +801,7 @@
             pl.when(s == v)(functools.partial(plane, v))
 
 
-START0, START1, HOP, CHUNK = 8.0, 6.3, 3.6, 0.88
+START0, START1, HOP, CHUNK = 8.4, 6.3, 3.6, 0.88
 FAR = 3.2
 MODES = ((0, 1, 1, 1), (0, 0, 1, 1))
 TOKENS = (10.5, 11.5, 12.5)

time: 51 us -> 50.8 us (level)
  no operation moved by 1% of the time
where the time goes in v4:
time: 50.8 us; the launch traced here: 50.6 us
  Pallas kernels  50 us (98%)
  local copies, waits for them, and re-layouts  0.66 us (1%)
    pallas_call x1, Pallas kernels, stationary(): pl.pallas_call(functools.partial(layer_kernel, n, nt, group), out_shape=p...  50 us

profile of v4, /device:TPU:0, one launch (start us, length us, event | category | flops | bytes accessed | tf_op | source)
XLA Modules:
  0.0 50.6 jit_solution(1106844417429760366)
XLA Ops:
  0.0 50.0 %layer.1 = bf16[32,2048]{1,0:T(8,128)(2,1)S(1)} custom-call(bf16[4,4,8,512]{3,2,1,0:T(8,128)(2,1)} %bitcast.4, f32[1,2048]{1,0:T(1,128)} %bitcast.5, bf16[256,512]{1,0:T(8,128)(2,1)} %aq_ref.1, bf16[128,512]{1,0:T(8,128)(2,1)} %ak_ref.1, bf16[128,512]{1,0:T(8,128)(2,1)} %av_ref.1, bf16[256,512]{1,0:T(8,128)(2,1)} %rq_ref.1, bf16[256,512]{1,0:T(8,128)(2,1)} %rf_ref.1, ...), custom_call_target="tpu_custom_call" | custom-call | tf_op jit(solution)/shard_map/layer/pallas_call | solution.py:847
  50.0 0.7 %copy.16 = bf16[32,2048]{1,0:T(8,128)(2,1)} copy(bf16[32,2048]{1,0:T(8,128)(2,1)S(1)} %layer.1) | data formatting | bytes 262144
